TPU v7x, 512 devices: a whole 4x4x16 slice. The times are simulated.
512 devices in a mesh: sp: 16 (over z), tp: 4 (over y), dp: 8 (over x, core).
Axes of the slice: x: 4, y: 4, z: 16, core: 2. Of those that a mesh axis runs over, the one named last changes fastest.
Arguments:
- latent: bfloat16 [8, 6144, 2048], P('dp', 'sp'), may hold values from -6 to 6
- conditioning: bfloat16 [8, 2048], P(None, 'sp'), may hold values from -6 to 6
- context_cond: bfloat16 [2048], P('sp'), may hold values from -6 to 6
- modulation: bfloat16 [3, 2048, 2048], P(None, 'sp', ('tp', 'dp')), may hold values from -4.2426407 to 4.2426407
- context: bfloat16 [8, 1024, 2048], P('dp', 'sp'), may hold values from -6 to 6
- query_weight: bfloat16 [2048, 1024], P(None, 'tp'), may hold values from -2.1213203 to 2.1213203
- key_projection: bfloat16 [2048, 256], P(None, 'tp'), may hold values from -0.13258252 to 0.13258252
- value_projection: bfloat16 [2048, 256], P(None, 'tp'), may hold values from -0.125 to 0.125
- out_weight: bfloat16 [1024, 2048], P(None, 'tp'), may hold values from -0.1875 to 0.1875
- sink_head_logit: float32 [16], P('tp'), may hold values from 5 to 7.5
- prefix_logit_bias: float32 [16], P('tp'), may hold values from -2.5 to -1
Outputs:
- updated: float32 [8, 6144, 2048], P('dp', 'sp', 'tp')
All inputs are finite; a program needn't handle non-finite values.
Results may differ from a plain program's by a relative error of at most 0.0073.
Values may be sent and summed in bfloat16 or wider, within the bound.
A program may use at most 64 MiB of HBM per device.

v0:
```python
import jax
import jax.numpy as jnp
from jax import lax
from jax.sharding import PartitionSpec as P

HEAD_SIZE = 64
GRID_W = 64
WINDOW_REACH = 128


NORM_EPSILON = 1e-06
ROTARY_BASE = 10000.0
MASKED = -1e30


def sent_to_all(value, axis):
    size = lax.axis_size(axis)
    return lax.all_to_all(
        jnp.broadcast_to(value[None], (size, *value.shape)), axis, 0, 0, tiled=True
    )


def over_copies(value, axis):
    everything = sent_to_all(value, axis)
    return jnp.sum(everything, axis=0)


def laid_out(pieces, dim):
    shape = list(pieces.shape[1:])
    shape[dim] *= pieces.shape[0]
    return jnp.moveaxis(pieces, 0, dim).reshape(shape)


def gathered_copies(value, axis, dim):
    pieces = sent_to_all(value, axis)
    return laid_out(pieces, dim)


def extended(value, sides, width):
    for axis, dim in sides:
        size, length = (lax.axis_size(axis), value.shape[dim])
        up = [(i, (i + 1) % size) for i in range(size - 1)]
        down = [(j, i) for i, j in up]
        last = lax.slice_in_dim(value, length - width, length, axis=dim)
        leading = lax.slice_in_dim(value, 0, width, axis=dim)
        before = lax.ppermute(last, axis, up)
        after = lax.ppermute(leading, axis, down)
        value = jnp.concatenate([before, value, after], axis=dim)
    return value


def layer_norm(tok_rows):
    vectors = tok_rows.astype(jnp.float32)
    centre = jnp.mean(vectors, axis=-1, keepdims=True)
    spread = jnp.mean(jnp.square(vectors - centre), axis=-1, keepdims=True)
    return (vectors - centre) * lax.rsqrt(spread + NORM_EPSILON)


def turn_half(segment, token_positions):
    half_width = segment.shape[-1]
    quarter = half_width // 2
    frequency = ROTARY_BASE ** (-jnp.arange(0, half_width, 2, dtype=jnp.float32) / half_width)
    angles = token_positions.astype(jnp.float32)[:, None] * frequency[None, :]
    cosine = jnp.cos(angles)[:, None, :]
    sine_table = jnp.sin(angles)[:, None, :]
    leading = segment[..., :quarter]
    trailing = segment[..., quarter:]
    return jnp.concatenate(
        [leading * cosine - trailing * sine_table, trailing * cosine + leading * sine_table],
        axis=-1,
    )


def apply_rotary(head_rows, token_positions):
    half_width = head_rows.shape[-1] // 2
    return jnp.concatenate(
        [
            turn_half(head_rows[..., :half_width], token_positions // GRID_W),
            turn_half(head_rows[..., half_width:], token_positions % GRID_W),
        ],
        axis=-1,
    )


def per_device(
    latent,
    conditioning,
    context_cond,
    modulation,
    context,
    query_weight,
    key_projection,
    value_projection,
    out_weight,
    sink_head_logit,
    prefix_logit_bias,
):
    sample = lax.axis_index("dp")
    samples = conditioning.shape[0]
    cond_rows = jnp.concatenate([conditioning, context_cond[None, :]], axis=0)
    activated = jax.nn.silu(cond_rows.astype(jnp.float32)).astype(jnp.bfloat16)
    partial_value = jnp.einsum(
        "sd,mdc->msc", activated, modulation, preferred_element_type=jnp.float32
    )
    summed = over_copies(partial_value, "sp")
    mod_all = gathered_copies(summed, ("tp", "dp"), 2)
    mod_shift = lax.dynamic_index_in_dim(mod_all[0], sample, 0, keepdims=False)
    mod_scale = lax.dynamic_index_in_dim(mod_all[1], sample, 0, keepdims=False)
    mod_gate = lax.dynamic_index_in_dim(mod_all[2], sample, 0, keepdims=False)
    ctx_shift = mod_all[0, samples]
    ctx_scale = mod_all[1, samples]
    ctx_normed = (layer_norm(context[0]) * (1.0 + ctx_scale) + ctx_shift).astype(jnp.bfloat16)
    prefix_keys = jnp.dot(ctx_normed, key_projection, preferred_element_type=jnp.float32).astype(
        jnp.bfloat16
    )
    prefix_values = jnp.dot(
        ctx_normed, value_projection, preferred_element_type=jnp.float32
    ).astype(jnp.bfloat16)
    context_pairs = gathered_copies(jnp.concatenate([prefix_keys, prefix_values], axis=1), "sp", 0)
    tok_rows = latent.shape[1]
    own_rows = latent[0]
    normalized_input = (layer_norm(own_rows) * (1.0 + mod_scale) + mod_shift).astype(jnp.bfloat16)
    offset = lax.axis_index("sp") * tok_rows
    token_positions = offset + jnp.arange(tok_rows, dtype=jnp.int32)
    local_heads = query_weight.shape[1] // HEAD_SIZE
    local_kv = key_projection.shape[1] // HEAD_SIZE
    heads_per_group = local_heads // local_kv
    kv_width = local_kv * HEAD_SIZE
    query_rows = apply_rotary(
        jnp.dot(normalized_input, query_weight, preferred_element_type=jnp.float32).reshape(
            tok_rows, local_heads, HEAD_SIZE
        ),
        token_positions,
    ).astype(jnp.bfloat16)
    key_token_rows = apply_rotary(
        jnp.dot(normalized_input, key_projection, preferred_element_type=jnp.float32).reshape(
            tok_rows, local_kv, HEAD_SIZE
        ),
        token_positions,
    ).astype(jnp.bfloat16)
    value_token_rows = jnp.dot(
        normalized_input, value_projection, preferred_element_type=jnp.float32
    ).astype(jnp.bfloat16)
    own_pairs = jnp.concatenate(
        [key_token_rows.reshape(tok_rows, kv_width), value_token_rows], axis=1
    )
    padded = extended(own_pairs, (("sp", 0),), WINDOW_REACH)
    block_list = tok_rows // WINDOW_REACH
    stacked = padded.reshape(block_list + 2, WINDOW_REACH, 2 * kv_width)
    window_pairs = jnp.concatenate([stacked[:-2], stacked[1:-1], stacked[2:]], axis=1)
    window_keys = window_pairs[..., :kv_width].reshape(
        block_list, 3 * WINDOW_REACH, local_kv, HEAD_SIZE
    )
    window_values = window_pairs[..., kv_width:].reshape(
        block_list, 3 * WINDOW_REACH, local_kv, HEAD_SIZE
    )
    context_keys = context_pairs[:, :kv_width].reshape(-1, local_kv, HEAD_SIZE)
    context_values = context_pairs[:, kv_width:].reshape(-1, local_kv, HEAD_SIZE)
    query_block_list = query_rows.reshape(
        block_list, WINDOW_REACH, local_kv, heads_per_group, HEAD_SIZE
    )
    block_start = jnp.arange(block_list, dtype=jnp.int32)[:, None] * WINDOW_REACH
    query_pos = block_start + jnp.arange(WINDOW_REACH, dtype=jnp.int32)[None, :]
    key_pos = block_start - WINDOW_REACH + jnp.arange(3 * WINDOW_REACH, dtype=jnp.int32)[None, :]
    global_key = key_pos + offset
    inside = (global_key >= 0) & (global_key < tok_rows * lax.axis_size("sp"))
    valid = (jnp.abs(query_pos[:, :, None] - key_pos[:, None, :]) <= WINDOW_REACH) & inside[
        :, None, :
    ]
    factor = HEAD_SIZE ** (-0.5)
    win_scores = (
        jnp.einsum(
            "nqkgd,njkd->nkgqj", query_block_list, window_keys, preferred_element_type=jnp.float32
        )
        * factor
    )
    win_scores = jnp.where(valid[:, None, None, :, :], win_scores, MASKED)
    head_bias_rows = prefix_logit_bias.reshape(local_kv, heads_per_group)[None, :, :, None, None]
    ctx_scores = (
        jnp.einsum(
            "nqkgd,ckd->nkgqc", query_block_list, context_keys, preferred_element_type=jnp.float32
        )
        * factor
        + head_bias_rows
    )
    sink_head_rows = sink_head_logit.reshape(local_kv, heads_per_group)[None, :, :, None]
    highest = jnp.maximum(
        jnp.maximum(jnp.max(win_scores, axis=-1), jnp.max(ctx_scores, axis=-1)), sink_head_rows
    )
    win_exp = jnp.exp(win_scores - highest[..., None])
    ctx_exp = jnp.exp(ctx_scores - highest[..., None])
    denominator = (
        jnp.sum(win_exp, axis=-1) + jnp.sum(ctx_exp, axis=-1) + jnp.exp(sink_head_rows - highest)
    )
    win_probs = (win_exp / denominator[..., None]).astype(jnp.bfloat16)
    ctx_probs = (ctx_exp / denominator[..., None]).astype(jnp.bfloat16)
    attended = jnp.einsum(
        "nkgqj,njkd->nqkgd", win_probs, window_values, preferred_element_type=jnp.float32
    )
    attended = attended + jnp.einsum(
        "nkgqc,ckd->nqkgd", ctx_probs, context_values, preferred_element_type=jnp.float32
    )
    attended = attended.astype(jnp.bfloat16).reshape(tok_rows, local_heads * HEAD_SIZE)
    col_width = out_weight.shape[1]
    mixed = jnp.dot(
        lax.all_gather(attended, "tp", axis=1, tiled=True),
        out_weight,
        preferred_element_type=jnp.float32,
    )
    col_start = lax.axis_index("tp") * col_width
    residual = lax.dynamic_slice_in_dim(own_rows, col_start, col_width, 1).astype(jnp.float32)
    gate_cols = lax.dynamic_slice_in_dim(mod_gate, col_start, col_width, 0)
    return (residual + gate_cols * mixed)[None]


def solution(mesh):
    placed = (
        P("dp", "sp", None),
        P(None, "sp"),
        P("sp"),
        P(None, "sp", ("tp", "dp")),
        P("dp", "sp", None),
        P(None, "tp"),
        P(None, "tp"),
        P(None, "tp"),
        P(None, "tp"),
        P("tp"),
        P("tp"),
    )
    return jax.shard_map(
        per_device, mesh=mesh, in_specs=placed, out_specs=P("dp", "sp", "tp"), check_vma=False
    )
```

profile of v0, /device:TPU:32, one launch (start us, length us, event | category | flops | bytes accessed | tf_op | source)
XLA Modules:
  0.0 112.0 jit_solution(2030573647287617)
XLA Ops:
  0.0 1.1 convolution_bitcast_fusion.2
  1.2 0.9 reshape.534
  2.1 15.2 %all-to-all-start = ((f32[16,1,1728]{2,1,0:T(1,128)}), f32[16,1,1728]{2,1,0:T(1,128)S(1)}, u32[]{:S(2)}, u32[]{:S(2)}) async-start(f32[16,1,1728]{2,1,0:T(1,128)} %reshape.534), calls=%async_computation | async-start | bytes 229376 | tf_op jit(solution)/shard_map/all_to_all | solution.py:18
  17.4 1.1 convert_reduce_fusion.1
  18.5 1.2 %fusion.40 = f32[64]{0:T(128)S(1)} fusion(bf16[1,64,2048]{2,1,0:T(8,128)(2,1)} %param.15, f32[64]{0:T(128)S(1)} %broadcast_multiply_fusion.1), kind=kLoop, calls=%fused_computation.55 | loop fusion | flops 524224 | bytes 262656 | tf_op jit(solution)/shard_map/reduce_sum | solution.py:55
  19.7 1.7 %convert_reduce_fusion = f32[384]{0:T(512)S(1)} fusion(bf16[1,384,2048]{2,1,0:T(8,128)(2,1)} %param.11), kind=kLoop, calls=%fused_computation.7 | loop fusion | flops 1572480 | bytes 1574400 | tf_op jit(solution)/shard_map/reduce_sum | solution.py:54
  21.5 0.6 copy-done.9
  22.6 0.6 add_rsqrt_fusion
  23.3 2.3 %copy.49 = bf16[2048,256]{0,1:T(8,128)(2,1)} copy(bf16[2048,256]{1,0:T(8,128)(2,1)} %param.16) | data formatting | bytes 2097152 | tf_op args[5]
  25.5 0.9 multiply_cosine_fusion
  26.9 3.9 %all-to-all-done = f32[16,1,1728]{2,1,0:T(1,128)S(1)} async-done(((f32[16,1,1728]{2,1,0:T(1,128)}), f32[16,1,1728]{2,1,0:T(1,128)S(1)}, u32[]{:S(2)}, u32[]{:S(2)}) %all-to-all-start) | async-done | bytes 110624 | tf_op jit(solution)/shard_map/all_to_all | solution.py:18
  30.9 0.6 broadcast.437
  31.5 0.9 reduce.6
  32.7 1.2 %reshape.536 = f32[32,1,1728]{2,1,0:T(1,128)} reshape(f32[32,9,3,64]{3,2,1,0:T(4,128)S(1)} %broadcast_bitcast_fusion) | data formatting | bytes 442368
  33.8 7.3 %all-to-all-start.1 = ((f32[32,1,1728]{2,1,0:T(1,128)}), f32[32,1,1728]{2,1,0:T(1,128)S(1)}, u32[]{:S(2)}, u32[]{:S(2)}) async-start(f32[32,1,1728]{2,1,0:T(1,128)} %reshape.536), calls=%async_computation.1 | async-start | bytes 458752 | tf_op jit(solution)/shard_map/all_to_all | solution.py:18
  41.7 7.9 %all-to-all-done.1 = f32[32,1,1728]{2,1,0:T(1,128)S(1)} async-done(((f32[32,1,1728]{2,1,0:T(1,128)}), f32[32,1,1728]{2,1,0:T(1,128)S(1)}, u32[]{:S(2)}, u32[]{:S(2)}) %all-to-all-start.1) | async-done | bytes 221216 | tf_op jit(solution)/shard_map/all_to_all | solution.py:18
  49.6 1.9 %reduce.7 = f32[32,1728]{1,0:T(8,128)} reduce(f32[32,1,1728]{2,1,0:T(1,128)S(1)} %all-to-all-done.1, f32[]{:T(128)} %broadcast.437), dimensions={1}, to_apply=%all_to_all.10.reduce_sub_computation | reduce | bytes 442372 | tf_op jit(solution)/shard_map/all_to_all | solution.py:18
  51.5 1.2 %reshape.537 = f32[32,9,3,64]{3,2,1,0:T(4,128)S(1)} reshape(f32[32,1728]{1,0:T(8,128)} %reduce.7) | data formatting | bytes 442368
  52.9 1.1 fusion.88
  53.9 0.9 reshape.522
  54.9 0.9 slice_add_fusion
  55.7 1.3 %convolution_convert_fusion.1 = bf16[64,64]{1,0:T(8,128)(2,1)S(1)} fusion(bf16[2048,64]{0,1:T(8,128)(2,1)} %param.18, bf16[1,64,2048]{2,1,0:T(8,128)(2,1)} %param.15, f32[2048]{0:T(1024)S(1)} %bitcast.232, f32[2048]{0:T(1024)S(1)} %bitcast.230, f32[64]{0:T(128)} %add_rsqrt_fusion.1, f32[64]{0:T(128)} %copy-done.16), kind=kOutput, calls=%fused_computation.46 | convolution fusion | flops 17567744 | bytes 549376 | tf_op jit(solution)/shard_map/dot_general | solution.py:116
  57.1 1.3 %convolution_convert_fusion.2 = bf16[64,64]{1,0:T(8,128)(2,1)S(1)} fusion(bf16[2048,64]{0,1:T(8,128)(2,1)} %param.17, bf16[1,64,2048]{2,1,0:T(8,128)(2,1)S(1)} %copy-done.4, f32[2048]{0:T(1024)S(1)} %bitcast.233, f32[2048]{0:T(1024)S(1)} %bitcast.231, f32[64]{0:T(128)} %add_rsqrt_fusion.1, f32[64]{0:T(128)} %copy-done.16), kind=kOutput, calls=%fused_computation.47 | convolution fusion | flops 17567744 | bytes 549376 | tf_op jit(solution)/shard_map/dot_general | solution.py:113
  58.4 0.9 copy.42
  59.4 0.9 copy.41
  60.5 0.8 broadcast_in_dim.23
  61.2 8.1 %all-to-all-start.2 = ((bf16[16,64,128]{2,1,0:T(8,128)(2,1)}), bf16[16,64,128]{2,1,0:T(8,128)(2,1)S(1)}, u32[]{:S(2)}, u32[]{:S(2)}) async-start(bf16[16,64,128]{2,1,0:T(8,128)(2,1)} %broadcast_in_dim.23), calls=%async_computation.2 | async-start | bytes 524288 | tf_op jit(solution)/shard_map/all_to_all | solution.py:18
  69.4 1.4 %fusion.8 = bf16[384,2048]{1,0:T(8,128)(2,1)S(1)} fusion(bf16[1,384,2048]{2,1,0:T(8,128)(2,1)S(1)} %copy-done.1, f32[2048]{0:T(1024)S(1)} %bitcast.228, f32[2048]{0:T(1024)S(1)} %bitcast.226, f32[384]{0:T(512)} %add_rsqrt_fusion, f32[384]{0:T(512)} %copy-done.9), kind=kLoop, calls=%fused_computation.15 | loop fusion | flops 4718592 | bytes 3165184 | tf_op jit(solution)/shard_map/convert_element_type | solution.py:122
  70.9 0.9 fusion.18
  71.9 0.6 convolution_bitcast_fusion.1
  73.3 0.6 fusion.35
  73.9 3.4 %collective-permute-start = (bf16[128,128]{0,1:T(8,128)(2,1)S(1)}, bf16[128,128]{0,1:T(8,128)(2,1)}, u32[]{:S(2)}, u32[]{:S(2)}) collective-permute-start(bf16[128,128]{0,1:T(8,128)(2,1)S(1)} %get-tuple-element.18), channel_id=1, source_target_pairs={{0,32},{32,64},{64,96},{96,128},{128,160},{160,192},{192,224},{224... | collective-permute-start | bytes 98312 | tf_op jit(solution)/shard_map/ppermute | solution.py:46
  77.3 3.2 %collective-permute-start.1 = (bf16[128,128]{0,1:T(8,128)(2,1)S(1)}, bf16[128,128]{0,1:T(8,128)(2,1)}, u32[]{:S(2)}, u32[]{:S(2)}) collective-permute-start(bf16[128,128]{0,1:T(8,128)(2,1)S(1)} %get-tuple-element.19), channel_id=1, source_target_pairs={{32,0},{64,32},{96,64},{128,96},{160,128},{192,160},{224,192},{256... | collective-permute-start | bytes 98312 | tf_op jit(solution)/shard_map/ppermute | solution.py:47
  80.6 0.7 copy.44
  81.3 0.7 copy.40
  82.0 1.0 squeeze.16
  83.0 1.6 %copy.47 = bf16[3,128,128]{1,2,0:T(8,128)(2,1)} copy(bf16[3,128,128]{2,1,0:T(8,128)(2,1)} %bitcast.223) | data formatting | bytes 196608 | tf_op jit(solution)/shard_map/slice | solution.py:150
  84.7 0.8 pad_maximum_fusion.2
  85.6 0.7 copy.46
  86.5 0.7 copy.48
  87.3 1.0 pad_maximum_fusion
  88.3 1.9 %fusion.16 = (f32[3,4,128]{2,1,0:T(4,128)S(1)}, f32[3,384,128,4]{2,1,3,0:T(8,128)}) fusion(pred[3,128,384]{1,2,0:T(8,128)(4,1)S(1)} %fusion.36, bf16[3,128,4,64]{1,3,2,0:T(8,128)(2,1)S(1)} %bitcast_dynamic-update-slice_fusion, bf16[3,384,128]{1,2,0:T(8,128)(2,1)S(1)} %pad_maximum_fusion), kind=kOutput, calls=%fused_computation.26 | convolution fusion | flops 77265408 | bytes 2856960 | tf_op jit(solution)/shard_map/nqkgd,njkd->nkgqj/dot_general | solution.py:172
  90.2 1.0 bitcast_reduce_fusion
  91.3 1.3 %fusion.1 = f32[3,4,128]{2,1,0:T(4,128)S(1)} fusion(f32[1024,3,128,4]{2,0,3,1:T(8,128)S(1)} %get-tuple-element.29, f32[3,4,128]{2,1,0:T(4,128)S(1)} %maximum_maximum_fusion, f32[4]{0:T(128)S(1)} %copy-done.14), kind=kLoop, calls=%fused_computation.5 | loop fusion | flops 6289920 | bytes 6303760 | tf_op jit(solution)/shard_map/reduce_sum | solution.py:193
  93.6 1.7 %fusion.27 = f32[3,128,1,4,64]{1,4,3,0,2:T(8,128)S(1)} fusion(f32[3,4,128]{2,1,0:T(4,128)S(1)} %exponential_add_fusion, f32[3,4,128]{2,1,0:T(4,128)S(1)} %maximum_maximum_fusion, f32[4]{0:T(128)S(1)} %copy-done.14, f32[1024,3,128,4]{2,0,3,1:T(8,128)S(1)} %get-tuple-element.29, bf16[1024,128]{1,0:T(8,128)(2,1)S(1)} %bitcast.219), kind=kOutput, calls=%fused_computation.38 | convolution fusion | flops 209190912 | bytes 6959120 | tf_op jit(solution)/shard_map/nkgqc,ckd->nqkgd/dot_general | solution.py:200
  95.3 0.7 fusion.32
  96.3 14.3 %all_gather.3 = bf16[384,1024]{0,1:T(8,128)(2,1)S(1)} all-gather(bf16[384,256]{0,1:T(8,128)(2,1)S(1)} %bitcast.222), channel_id=1, replica_groups=mesh['sp'=16,'tp'=4,'dp'=8] {'tp'}, dimensions={1}, use_global_device_ids=true | all-gather | bytes 983040 | tf_op jit(solution)/shard_map/all_gather | solution.py:206
  110.6 1.5 %fusion.25 = f32[1,384,512]{2,1,0:T(8,128)} fusion(bf16[384,1024]{0,1:T(8,128)(2,1)S(1)} %all_gather.3, bf16[1024,512]{1,0:T(8,128)(2,1)S(1)} %copy-done, f32[512]{0:T(512)S(1)} %bitcast.234, bf16[1,384,2048]{2,1,0:T(8,128)(2,1)S(1)} %copy-done.1, s32[]{:T(128)S(6)} %select_n.41), kind=kOutput, calls=%fused_computation.35 | convolution fusion | flops 403243008 | bytes 3016708 | tf_op jit(solution)/shard_map/dot_general | solution.py:205
  (77 shorter events, 5.1 us)
Async XLA Ops:
  0.0 110.5 %copy-start = (bf16[1024,512]{1,0:T(8,128)(2,1)S(1)}, bf16[1024,512]{1,0:T(8,128)(2,1)}, u32[]{:S(2)}) copy-start(bf16[1024,512]{1,0:T(8,128)(2,1)} %param.19) | copy-start | bytes 3145732
  0.0 22.0 %copy-start.1 = (bf16[1,384,2048]{2,1,0:T(8,128)(2,1)S(1)}, bf16[1,384,2048]{2,1,0:T(8,128)(2,1)}, u32[]{:S(2)}) copy-start(bf16[1,384,2048]{2,1,0:T(8,128)(2,1)} %param.11) | copy-start | bytes 4718596
  2.1 28.8 %all-to-all-start = ((f32[16,1,1728]{2,1,0:T(1,128)}), f32[16,1,1728]{2,1,0:T(1,128)S(1)}, u32[]{:S(2)}, u32[]{:S(2)}) async-start(f32[16,1,1728]{2,1,0:T(1,128)} %reshape.534), calls=%async_computation | async-start | bytes 229376 | tf_op jit(solution)/shard_map/all_to_all | solution.py:18
  17.3 9.1 %copy-start.11 = (f32[16]{0:T(128)}, f32[16]{0:T(128)S(1)}, u32[]{:S(2)}) copy-start(f32[16]{0:T(128)S(1)} %multiply_power_fusion) | copy-start | bytes 196
  18.5 7.9 %copy-start.16 = (f32[64]{0:T(128)}, f32[64]{0:T(128)S(1)}, u32[]{:S(2)}) copy-start(f32[64]{0:T(128)S(1)} %broadcast_multiply_fusion.1) | copy-start | bytes 772
  21.4 0.6 copy-start.9
  33.8 15.8 %all-to-all-start.1 = ((f32[32,1,1728]{2,1,0:T(1,128)}), f32[32,1,1728]{2,1,0:T(1,128)S(1)}, u32[]{:S(2)}, u32[]{:S(2)}) async-start(f32[32,1,1728]{2,1,0:T(1,128)} %reshape.536), calls=%async_computation.1 | async-start | bytes 458752 | tf_op jit(solution)/shard_map/all_to_all | solution.py:18
  52.8 4.3 %copy-start.4 = (bf16[1,64,2048]{2,1,0:T(8,128)(2,1)S(1)}, bf16[1,64,2048]{2,1,0:T(8,128)(2,1)}, u32[]{:S(2)}) copy-start(bf16[1,64,2048]{2,1,0:T(8,128)(2,1)} %param.15) | copy-start | bytes 786436
  57.1 13.7 %copy-start.10 = (f32[384]{0:T(512)S(1)}, f32[384]{0:T(512)}, u32[]{:S(2)}) copy-start(f32[384]{0:T(512)} %copy-done.9) | copy-start | bytes 4612
  57.1 13.7 %copy-start.13 = (f32[384]{0:T(512)S(1)}, f32[384]{0:T(512)}, u32[]{:S(2)}) copy-start(f32[384]{0:T(512)} %add_rsqrt_fusion) | copy-start | bytes 4612
  61.2 29.0 %all-to-all-start.2 = ((bf16[16,64,128]{2,1,0:T(8,128)(2,1)}), bf16[16,64,128]{2,1,0:T(8,128)(2,1)S(1)}, u32[]{:S(2)}, u32[]{:S(2)}) async-start(bf16[16,64,128]{2,1,0:T(8,128)(2,1)} %broadcast_in_dim.23), calls=%async_computation.2 | async-start | bytes 524288 | tf_op jit(solution)/shard_map/all_to_all | solution.py:18
  69.3 1.5 %copy-start.3 = (bf16[2048,256]{0,1:T(8,128)(2,1)S(1)}, bf16[2048,256]{0,1:T(8,128)(2,1)}, u32[]{:S(2)}) copy-start(bf16[2048,256]{0,1:T(8,128)(2,1)} %copy.49) | copy-start | bytes 3145732
  70.8 1.0 copy-start.8
  70.8 1.1 copy-start.7
  70.8 1.7 %copy-start.12 = (f32[16]{0:T(128)S(1)}, f32[16]{0:T(128)}, u32[]{:S(2)}) copy-start(f32[16]{0:T(128)} %copy-done.11) | copy-start | bytes 196
  70.8 2.4 %copy-start.6 = (bf16[2048,64]{0,1:T(8,128)(2,1)S(1)}, bf16[2048,64]{0,1:T(8,128)(2,1)}, u32[]{:S(2)}) copy-start(bf16[2048,64]{0,1:T(8,128)(2,1)} %param.18) | copy-start | bytes 786436
  71.8 9.5 %copy-start.5 = (f32[1,9,32,64]{3,0,1,2:T(1,128)S(1)}, f32[1,9,32,64]{3,0,1,2:T(1,128)}, u32[]{:S(2)}) copy-start(f32[1,9,32,64]{3,0,1,2:T(1,128)} %get-tuple-element.5) | copy-start | bytes 221188
  73.9 16.4 %copy-start.14 = (f32[4]{0:T(128)S(1)}, f32[4]{0:T(128)}, u32[]{:S(2)}) copy-start(f32[4]{0:T(128)} %param.21) | copy-start | bytes 52
  73.9 10.8 %collective-permute-start = (bf16[128,128]{0,1:T(8,128)(2,1)S(1)}, bf16[128,128]{0,1:T(8,128)(2,1)}, u32[]{:S(2)}, u32[]{:S(2)}) collective-permute-start(bf16[128,128]{0,1:T(8,128)(2,1)S(1)} %get-tuple-element.18), channel_id=1, source_target_pairs={{0,32},{32,64},{64,96},{96,128},{128,160},{160,192},{192,224},{224... | collective-permute-start | bytes 98312 | tf_op jit(solution)/shard_map/ppermute | solution.py:46
  77.3 7.4 %collective-permute-start.1 = (bf16[128,128]{0,1:T(8,128)(2,1)S(1)}, bf16[128,128]{0,1:T(8,128)(2,1)}, u32[]{:S(2)}, u32[]{:S(2)}) collective-permute-start(bf16[128,128]{0,1:T(8,128)(2,1)S(1)} %get-tuple-element.19), channel_id=1, source_target_pairs={{32,0},{64,32},{96,64},{128,96},{160,128},{192,160},{224,192},{256... | collective-permute-start | bytes 98312 | tf_op jit(solution)/shard_map/ppermute | solution.py:47
  90.2 1.0 copy-start.15
  91.3 1.7 %copy-start.2 = (f32[3,384,128,4]{2,1,3,0:T(8,128)S(1)}, f32[3,384,128,4]{2,1,3,0:T(8,128)}, u32[]{:S(2)}) copy-start(f32[3,384,128,4]{2,1,3,0:T(8,128)} %get-tuple-element.27) | copy-start | bytes 7077892
where the time goes:
time: 113 us; the launch traced here: 112 us
  starting transfers between devices  37.2 us (33%)
  local copies, waits for them, and re-layouts  18.5 us (16%)
  other arithmetic  17 us (15%)
  blocking collectives  14.3 us (13%)
  matrix products  12.7 us (11%)
  waiting for transfers between devices  11.9 us (11%)
    all_to_all x3, starting transfers between devices, sent_to_all(): lax.all_to_all(jnp.broadcast_to(value[None], (size, *value.shape)), axis,...  30.6 us
    all_gather x1, blocking collectives, per_device(): lax.all_gather(attended, 'tp', axis=1, tiled=True)  14.3 us
    all_to_all x3, waiting for transfers between devices, sent_to_all(): lax.all_to_all(jnp.broadcast_to(value[None], (size, *value.shape)), axis,...  11.9 us
    unnamed x45, local copies, waits for them, and re-layouts  6.88 us
    ppermute x1, starting transfers between devices, extended(): before = lax.ppermute(last, axis, up)  3.37 us
    ppermute x1, starting transfers between devices, extended(): after = lax.ppermute(leading, axis, down)  3.23 us
    reduce_sum x2, other arithmetic, layer_norm(): centre = jnp.mean(vectors, axis=-1, keepdims=True)  2.79 us
    all_to_all x2, other arithmetic, sent_to_all(): lax.all_to_all(jnp.broadcast_to(value[None], (size, *value.shape)), axis,...  2.78 us
  transfers between devices with their start and end apart: 5, of which 2 were waited for; matrix products, arithmetic and copies ran while one was open for 21% of the time, Pallas kernels for 0%

commit v1 on v0

v1 whole, which is shorter than its diff:
```python
import functools
import math

import jax
import jax.numpy as jnp
from jax import lax
from jax.experimental import pallas as pl
from jax.experimental.pallas import tpu as pltpu
from jax.sharding import PartitionSpec as P

HEAD = 64
GRID_W = 64
REACH = 128
EPS = 1e-06
BASE = 10000.0
MASKED = -1e30
LOG2E = math.log2(math.e)
F32 = jnp.float32
BF16 = jnp.bfloat16
LANES = 128
MESH = pl.DeviceIdType.MESH


def dot(a, b):
    return jnp.dot(a, b, preferred_element_type=F32)


def dot_t(a, b):
    return lax.dot_general(a, b, (((1,), (1,)), ((), ())), preferred_element_type=F32)


def lane_iota(shape):
    return lax.broadcasted_iota(jnp.int32, shape, len(shape) - 1)


def kernel(
    sizes,
    lat, cond, cctx, mod, ctx, qw, kw, vw, ow, sink, bias,
    out,
    xv, condv, cctxv, modv, cxv, qwv, kwv, vwv, owv, sinks, biass,
    zsend, zrecv, xysend, xyrecv, vecs,
    xn, cxn, xb, cxb, kvw, ct, st,
    kvc, kvx, qz, accw, mw, gath, outv,
    in_sems, out_sem,
    z_send, z_recv, xy_send, xy_recv, c_send, c_recv, h_send, h_recv, y_send, y_recv,
):
    SP, TP, DP = sizes
    T, D = xv.shape
    C = cxv.shape[0]
    samples = condv.shape[0]
    cols = owv.shape[1]
    width = qwv.shape[1]
    heads = width // HEAD
    blocks = T // REACH
    sp, tp, dp = lax.axis_index("sp"), lax.axis_index("tp"), lax.axis_index("dp")

    barrier = pltpu.get_barrier_semaphore()
    z_far = sorted(range(1, SP), key=lambda d: -min(d, SP - d))
    xy_off = [(t, d) for t in range(TP) for d in range(DP) if (t, d) != (0, 0)]
    for d in z_far:
        pl.semaphore_signal(barrier, inc=1, device_id={"sp": lax.rem(sp + d, SP)}, device_id_type=MESH)
    for t, d in xy_off:
        pl.semaphore_signal(
            barrier, inc=1, device_id={"tp": lax.rem(tp + t, TP), "dp": lax.rem(dp + d, DP)}, device_id_type=MESH
        )

    pairs = [(cond, condv), (cctx, cctxv), (mod, modv), (lat, xv), (ctx, cxv), (kw, kwv), (vw, vwv), (qw, qwv),
             (ow, owv), (sink, sinks), (bias, biass)]
    loads = []
    for i, (src, dst) in enumerate(pairs):
        copy = pltpu.make_async_copy(src, dst, in_sems.at[i])
        copy.start()
        loads.append(copy)

    loads[0].wait()
    loads[1].wait()
    loads[2].wait()
    act = jax.nn.silu(condv[...].astype(F32)).astype(BF16)
    act_c = jax.nn.silu(jnp.broadcast_to(cctxv[...].astype(F32), (8, cctxv.shape[1]))).astype(BF16)

    def packed(m):
        return dot(act, modv[m]), dot(act_c, modv[m])

    s0, c0 = packed(0)
    s1, c1 = packed(1)
    g2 = dot(act, modv[2])
    half = samples // 2
    main = jnp.concatenate([s0, s1], axis=1)
    side = jnp.concatenate([c0, c1], axis=1)
    gates = jnp.concatenate([g2[:half], g2[half:]], axis=1)
    zsend[0:samples, :] = main.astype(BF16)
    zsend[8:16, :] = jnp.concatenate([side[0:8 - half], gates], axis=0).astype(BF16)

    pl.semaphore_wait(barrier, len(z_far) + len(xy_off))

    sends = []
    for d in z_far:
        copy = pltpu.make_async_remote_copy(
            src_ref=zsend, dst_ref=zrecv.at[d - 1], send_sem=z_send, recv_sem=z_recv,
            device_id={"sp": lax.rem(sp + d, SP)}, device_id_type=MESH,
        )
        copy.start()

    loads[3].wait()

    def norm_rows(src, dst, rows):
        def step(i, _):
            r = pl.ds(pl.multiple_of(i * rows, rows), rows)
            v = src[r, :].astype(F32)
            v = v - jnp.mean(v, axis=-1, keepdims=True)
            dst[r, :] = v * lax.rsqrt(jnp.mean(v * v, axis=-1, keepdims=True) + EPS)
            return 0

        lax.fori_loop(0, src.shape[0] // rows, step, 0)

    norm_rows(xv, xn, 16)
    loads[4].wait()
    norm_rows(cxv, cxn, 16)
    loads[5].wait()
    loads[6].wait()
    kvw[...] = jnp.concatenate([kwv[...], vwv[...]], axis=1)
    kvc[:, LANES:] = jnp.ones((kvc.shape[0], LANES), BF16)
    kvx[:, LANES:] = jnp.ones((kvx.shape[0], LANES), BF16)

    lane = lane_iota((T, LANES))
    pos = lax.broadcasted_iota(jnp.int32, (T, LANES), 0) + sp * T
    inner = lane & 31
    freq = jnp.exp((inner & 15).astype(F32) * (-2.0 / 32.0 * math.log(BASE)))
    place = jnp.where((lane & 63) < 32, pos >> 6, pos & 63).astype(F32)
    angle = place * freq
    ct[...] = jnp.cos(angle)
    sine = jnp.sin(angle)
    st[...] = jnp.where(inner < 16, -sine, sine)

    pltpu.make_async_copy(zrecv, zrecv, z_recv).wait()
    total = zsend[...].astype(F32)
    for d in range(SP - 1):
        total = total + zrecv[d].astype(F32)
    odd = lax.rem(dp, 2)
    turned = pltpu.roll(total, 64, 1)
    here = jnp.where(odd == 0, total, turned)
    there = jnp.where(odd == 0, turned, total)
    keep = (lane_iota(total.shape) >> 6) == odd
    here = jnp.where(keep, here, 0.0)
    there = jnp.where(keep, there, 0.0)
    first_gate = 8 + 8 - half
    for s in range(samples):
        gate_rows = here if s < half else there
        row = first_gate + s % half
        xysend[s, 0:1, :] = here[s:s + 1]
        xysend[s, 1:2, :] = there[s:s + 1]
        xysend[s, 2:3, :] = here[8:9]
        xysend[s, 3:4, :] = there[8:9]
        xysend[s, 4:5, :] = gate_rows[row:row + 1]
    me = tp * DP + dp
    for t, d in xy_off:
        target = lax.rem(dp + d, DP)
        copy = pltpu.make_async_remote_copy(
            src_ref=xysend.at[target], dst_ref=xyrecv.at[me], send_sem=xy_send, recv_sem=xy_recv,
            device_id={"tp": lax.rem(tp + t, TP), "dp": target}, device_id_type=MESH,
        )
        copy.start()
    xyrecv[me] = xysend[dp]
    others = xyrecv.at[pl.ds(0, len(xy_off))]
    pltpu.make_async_copy(others, others, xy_recv).wait()
    chunks = vecs.shape[0]
    extra = jnp.where(lax.broadcasted_iota(jnp.int32, (8, LANES), 0) % 2 == 1, 1.0, 0.0)
    for k in range(chunks):
        vecs[k] = xyrecv[2 * k] + xyrecv[2 * k + 1] + extra

    def modulate(src, dst, shift_row):
        def step(k, _):
            c = pl.ds(pl.multiple_of(k * LANES, LANES), LANES)
            shift = vecs[k, shift_row:shift_row + 1, :]
            scale = vecs[k, shift_row + 1:shift_row + 2, :]
            dst[:, c] = (src[:, c] * scale + shift).astype(BF16)
            return 0

        lax.fori_loop(0, chunks, step, 0)

    modulate(cxn, cxb, 2)
    kvc[0:C, 0:LANES] = dot(cxb[...], kvw[...]).astype(BF16)
    for d in z_far:
        copy = pltpu.make_async_remote_copy(
            src_ref=kvc.at[pl.ds(0, C), pl.ds(0, LANES)], dst_ref=kvc.at[pl.ds(d * C, C), pl.ds(0, LANES)],
            send_sem=c_send, recv_sem=c_recv, device_id={"sp": lax.rem(sp + d, SP)}, device_id_type=MESH,
        )
        copy.start()

    modulate(xn, xb, 0)

    def partner(v):
        low = (lane_iota(v.shape) & 31) < 16
        return jnp.where(low, pltpu.roll(v, LANES - 16, 1), pltpu.roll(v, 16, 1))

    kv = dot(xb[...], kvw[...])
    is_key = lane_iota((T, LANES)) < 64
    kv = jnp.where(is_key, kv * ct[...] + partner(kv) * st[...], kv)
    kvx[REACH:REACH + T, 0:LANES] = kv.astype(BF16)
    before, after = lax.rem(sp + SP - 1, SP), lax.rem(sp + 1, SP)
    for side_index, (at, to, there_at) in enumerate(((T, after, 0), (REACH, before, REACH + T))):
        copy = pltpu.make_async_remote_copy(
            src_ref=kvx.at[pl.ds(at, REACH), pl.ds(0, LANES)], dst_ref=kvx.at[pl.ds(there_at, REACH), pl.ds(0, LANES)],
            send_sem=h_send.at[side_index], recv_sem=h_recv.at[side_index], device_id={"sp": to}, device_id_type=MESH,
        )
        copy.start()
        sends.append(copy)

    loads[7].wait()
    factor = LOG2E * HEAD ** (-0.5)
    low_lane = lane_iota((T, LANES)) < 64
    for j in range(width // LANES):
        q = dot(xb[...], qwv[:, j * LANES:(j + 1) * LANES])
        q = (q * ct[...] + partner(q) * st[...]) * factor
        qz[2 * j] = jnp.where(low_lane, q, 0.0).astype(BF16)
        qz[2 * j + 1] = jnp.where(low_lane, pltpu.roll(q, 64, 1), 0.0).astype(BF16)

    loads[9].wait()
    loads[10].wait()

    def per_head(ref):
        return jnp.concatenate([jnp.full((REACH, 1), ref[h] * LOG2E, F32) for h in range(heads)], axis=0)

    for copy in sends:
        copy.wait_recv()

    def window(b, _):
        r = pl.multiple_of(b * REACH, REACH)
        q = qz[:, pl.ds(r, REACH), :].reshape(heads * REACH, LANES)
        keys = kvx[pl.ds(r, 3 * REACH), :]
        s = dot_t(q, keys[:, 0:LANES])
        i = lax.broadcasted_iota(jnp.int32, (REACH, 3 * REACH), 0)
        j = lax.broadcasted_iota(jnp.int32, (REACH, 3 * REACH), 1)
        where = sp * T + r - REACH + j
        valid = (j >= i) & (j <= i + 2 * REACH) & (where >= 0) & (where < SP * T)
        s = jnp.where(valid[None], s.reshape(heads, REACH, 3 * REACH), MASKED).reshape(heads * REACH, 3 * REACH)
        m = jnp.max(s, axis=1, keepdims=True)
        accw[b] = dot(jnp.exp2(s - m).astype(BF16), keys)
        mw[b] = jnp.broadcast_to(m, (heads * REACH, LANES))
        return 0

    lax.fori_loop(0, blocks, window, 0)

    others = kvc.at[pl.ds(C, (SP - 1) * C), pl.ds(0, LANES)]
    pltpu.make_async_copy(others, others, c_recv).wait()

    def tp_copy(b, t, start):
        rows = pl.ds(b * REACH if isinstance(b, int) else pl.multiple_of(b * REACH, REACH), REACH)
        return pltpu.make_async_remote_copy(
            src_ref=gath.at[tp, rows], dst_ref=gath.at[tp, rows], send_sem=y_send.at[b, t - 1],
            recv_sem=y_recv.at[b, t - 1], device_id={"tp": lax.rem(tp + t, TP)}, device_id_type=MESH,
        )

    def context(b, _):
        r = pl.multiple_of(b * REACH, REACH)
        q = qz[:, pl.ds(r, REACH), :].reshape(heads * REACH, LANES)
        s = dot_t(q, kvc[:, 0:LANES])
        bias2 = per_head(biass)
        sink2 = per_head(sinks)
        m0 = mw[b][:, 0:1]
        m = jnp.maximum(jnp.maximum(m0, sink2), jnp.max(s, axis=1, keepdims=True) + bias2)
        acc = dot(jnp.exp2(s - (m - bias2)).astype(BF16), kvc[...])
        acc = acc + accw[b] * jnp.exp2(m0 - m)
        att = acc[:, 0:LANES] / (acc[:, LANES:] + jnp.exp2(sink2 - m))
        att = att.reshape(heads, REACH, LANES)
        low = lane_iota((REACH, LANES)) < 64
        for j in range(heads // 2):
            pair = jnp.where(low, pltpu.roll(att[2 * j], 64, 1), att[2 * j + 1])
            gath[tp, pl.ds(r, REACH), j * LANES:(j + 1) * LANES] = pair.astype(BF16)
        for t in range(1, TP):
            tp_copy(b, t, True).start()
        return 0

    lax.fori_loop(0, blocks, context, 0)

    loads[8].wait()
    gate = jnp.concatenate([vecs[tp * (cols // LANES) + j, 4:5, :] for j in range(cols // LANES)], axis=1)

    def project(b, _):
        r = pl.multiple_of(b * REACH, REACH)
        rows = pl.ds(r, REACH)
        for t in range(1, TP):
            tp_copy(b, t, False).wait_recv()
        mixed = dot(gath[0, rows, :], owv[0:width, :])
        for t in range(1, TP):
            mixed = mixed + dot(gath[t, rows, :], owv[t * width:(t + 1) * width, :])
        own = xv[rows, pl.ds(pl.multiple_of(tp * cols, LANES), cols)].astype(F32)
        outv[rows, :] = own + gate * mixed
        pltpu.make_async_copy(outv.at[rows], out.at[rows], out_sem.at[b]).start()
        return 0

    lax.fori_loop(0, blocks, project, 0)

    for b in range(blocks):
        pltpu.make_async_copy(outv.at[pl.ds(b * REACH, REACH)], out.at[pl.ds(b * REACH, REACH)], out_sem.at[b]).wait()
        for t in range(1, TP):
            tp_copy(b, t, False).wait_send()
    for copy in sends:
        copy.wait_send()
    pltpu.make_async_copy(zrecv, zrecv, z_send).wait()
    others = xyrecv.at[pl.ds(0, len(xy_off))]
    pltpu.make_async_copy(others, others, xy_send).wait()
    others = kvc.at[pl.ds(C, (SP - 1) * C), pl.ds(0, LANES)]
    pltpu.make_async_copy(others, others, c_send).wait()


def per_device(sizes, lat, cond, cctx, mod, ctx, qw, kw, vw, ow, sink, bias):
    SP, TP, DP = sizes
    T, D = lat.shape[1:]
    C = ctx.shape[1]
    width = qw.shape[1]
    heads = width // HEAD
    blocks = T // REACH
    cols = ow.shape[1]
    samples = cond.shape[0]
    any_space = pl.BlockSpec(memory_space=pl.ANY)
    vmem = pltpu.VMEM
    dma = pltpu.SemaphoreType.DMA
    scratch = [
        vmem((T, D), BF16), vmem(cond.shape, BF16), vmem((1, cctx.shape[0]), BF16), vmem(mod.shape, BF16),
        vmem((C, D), BF16), vmem(qw.shape, BF16), vmem(kw.shape, BF16), vmem(vw.shape, BF16), vmem(ow.shape, BF16),
        pltpu.SMEM(sink.shape, F32), pltpu.SMEM(bias.shape, F32),
        vmem((16, LANES), BF16), vmem((SP - 1, 16, LANES), BF16),
        vmem((samples, 8, LANES), F32), vmem((TP * DP, 8, LANES), F32), vmem((TP * DP // 2, 8, LANES), F32),
        vmem((T, D), F32), vmem((C, D), F32), vmem((T, D), BF16), vmem((C, D), BF16), vmem((D, LANES), BF16),
        vmem((T, LANES), F32), vmem((T, LANES), F32),
        vmem((SP * C, 2 * LANES), BF16), vmem((T + 2 * REACH, 2 * LANES), BF16), vmem((heads, T, LANES), BF16),
        vmem((blocks, heads * REACH, 2 * LANES), F32), vmem((blocks, heads * REACH, LANES), F32),
        vmem((TP, T, width), BF16), vmem((T, cols), F32),
        dma((11,)), dma((blocks,)),
        dma, dma, dma, dma, dma, dma, dma((2,)), dma((2,)), dma((blocks, TP - 1)), dma((blocks, TP - 1)),
    ]
    result = pl.pallas_call(
        functools.partial(kernel, sizes),
        out_shape=jax.ShapeDtypeStruct((T, cols), F32),
        in_specs=[any_space] * 11,
        out_specs=any_space,
        scratch_shapes=scratch,
        compiler_params=pltpu.CompilerParams(
            collective_id=0, has_side_effects=True, vmem_limit_bytes=60 * 1024 * 1024
        ),
        name="step",
    )(lat[0], cond, cctx[None, :], mod, ctx[0], qw, kw, vw, ow, sink, bias)
    return result[None]


def solution(mesh):
    placed = (
        P("dp", "sp", None),
        P(None, "sp"),
        P("sp"),
        P(None, "sp", ("tp", "dp")),
        P("dp", "sp", None),
        P(None, "tp"),
        P(None, "tp"),
        P(None, "tp"),
        P(None, "tp"),
        P("tp"),
        P("tp"),
    )
    sizes = (mesh.shape["sp"], mesh.shape["tp"], mesh.shape["dp"])
    return jax.shard_map(
        functools.partial(per_device, sizes),
        mesh=mesh, in_specs=placed, out_specs=P("dp", "sp", "tp"), check_vma=False,
    )
```

time: 113 us -> 68.2 us (0.60)
  the two profiles are of different devices: /device:TPU:32 before, /device:TPU:1 now
where the time goes in v1:
time: 68.2 us; the launch traced here: 67.9 us
  Pallas kernels  60.4 us (89%)
  local copies, waits for them, and re-layouts  7.5 us (11%)
    pallas_call x1, Pallas kernels, per_device(): pl.pallas_call(functools.partial(kernel, sizes), out_shape=jax.ShapeDtype...  60.4 us
    unnamed x4, local copies, waits for them, and re-layouts  7.5 us

profile of v1, /device:TPU:1, one launch (start us, length us, event | category | flops | bytes accessed | tf_op | source)
XLA Modules:
  0.0 67.9 jit_solution(5052454799772363328)
XLA Ops:
  0.0 1.5 %copy.12.mod = bf16[3,128,64]{2,1,0:T(8,128)(2,1)} copy(bf16[3,128,64]{1,2,0:T(8,128)(2,1)} %param.14) | data formatting | bytes 98304 | tf_op args[3]
  1.5 2.0 %copy.13.kw = bf16[2048,64]{1,0:T(8,128)(2,1)} copy(bf16[2048,64]{0,1:T(8,128)(2,1)} %param.17) | data formatting | bytes 524288 | tf_op args[6]
  3.5 2.0 %copy.14.vw = bf16[2048,64]{1,0:T(8,128)(2,1)} copy(bf16[2048,64]{0,1:T(8,128)(2,1)} %param.18) | data formatting | bytes 524288 | tf_op args[7]
  5.4 60.4 %step.1 = f32[384,512]{1,0:T(8,128)} custom-call(bf16[384,2048]{1,0:T(8,128)(2,1)} %bitcast.5, bf16[8,128]{1,0:T(8,128)(2,1)} %cond.1, bf16[1,128]{1,0:T(2,128)(2,1)} %bitcast.7, bf16[3,128,64]{2,1,0:T(8,128)(2,1)} %copy.12.mod, bf16[64,2048]{1,0:T(8,128)(2,1)} %bitcast.6, bf16[2048,256]{1,0:T(8,128)(2,1)} %qw.1, bf16[2048,64]{1,0:T(8,128)(2,1)} %copy.13.kw, ...), custom_call_target="tpu_custom_call" | custom-call | tf_op jit(solution)/shard_map/step/pallas_call | solution.py:333
  65.9 2.1 %copy.16 = f32[1,384,512]{2,1,0:T(8,128)} copy(f32[1,384,512]{2,1,0:T(8,128)} %bitcast.4) | data formatting | bytes 1572864

commit v2 on v1

v2 whole, which is shorter than its diff:
```python
import functools
import math

import jax
import jax.numpy as jnp
from jax import lax
from jax.experimental import pallas as pl
from jax.experimental.pallas import tpu as pltpu
from jax.sharding import PartitionSpec as P

HEAD = 64
GRID_W = 64
REACH = 128
EPS = 1e-06
BASE = 10000.0
MASKED = -1e30
LOG2E = math.log2(math.e)
F32 = jnp.float32
BF16 = jnp.bfloat16
LANES = 128
MESH = pl.DeviceIdType.MESH


def dot(a, b):
    return jnp.dot(a, b, preferred_element_type=F32)


def dot_t(a, b):
    return lax.dot_general(a, b, (((1,), (1,)), ((), ())), preferred_element_type=F32)


def full(v):
    return jnp.broadcast_to(v, (v.shape[0], LANES))


def wide(v, width):
    return jnp.concatenate([v] * (width // LANES), axis=1)


def lane_iota(shape):
    return lax.broadcasted_iota(jnp.int32, shape, len(shape) - 1)


DIRECT = (5, -5, 1, -1, 2, -2, -3)
RELAYED = (3, 4, 6, 7, 8, -4, -6, -7)
SLOT = {0: 0, **{d: i + 1 for i, d in enumerate((1, -1, 2, -2, -3, 5, -5) + RELAYED)}}
NEAR = 5


def kernel(
    sizes,
    lat, cond, cctx, mod, ctx, qw, kw, vw, ow, sink, bias,
    out,
    xv, condv, cctxv, modv, cxv, qwv, owv, sinks, biass,
    zsend, zrecv, xysend, xyrecv, vecs,
    xn, cxn, xb, cxb, kvw, ct, st,
    kvc, kvx, qz, accw, mw, gath, outv,
    in_sems, out_sem,
    z_send, z_recv, xy_send, xy_recv, c_send, c_recv, h_send, h_recv, y_send, y_recv,
):
    SP, TP, DP = sizes
    T, D = xv.shape
    C = cxv.shape[0]
    samples = condv.shape[0]
    cols = owv.shape[1]
    width = qwv.shape[1]
    heads = width // HEAD
    blocks = T // REACH
    sp, tp, dp = lax.axis_index("sp"), lax.axis_index("tp"), lax.axis_index("dp")

    def z_at(d):
        return {"sp": lax.rem(sp + d + SP, SP)}

    barrier = pltpu.get_barrier_semaphore()
    z_far = sorted(range(1, SP), key=lambda d: -min(d, SP - d))
    xy_off = [(t, d) for t in range(TP) for d in range(DP) if (t, d) != (0, 0)]
    for d in z_far:
        pl.semaphore_signal(barrier, inc=1, device_id=z_at(d), device_id_type=MESH)
    for t, d in xy_off:
        pl.semaphore_signal(
            barrier, inc=1, device_id={"tp": lax.rem(tp + t, TP), "dp": lax.rem(dp + d, DP)}, device_id_type=MESH
        )

    pairs = [(cond, condv), (cctx, cctxv), (mod, modv), (lat, xv), (ctx, cxv), (kw, kvw.at[0:HEAD]),
             (vw, kvw.at[HEAD:LANES]), (qw, qwv), (ow, owv), (sink, sinks), (bias, biass)]
    loads = []
    for i, (src, dst) in enumerate(pairs):
        copy = pltpu.make_async_copy(src, dst, in_sems.at[i])
        copy.start()
        loads.append(copy)

    loads[0].wait()
    loads[1].wait()
    loads[2].wait()
    act = jax.nn.silu(condv[...].astype(F32)).astype(BF16)
    act_c = jax.nn.silu(jnp.broadcast_to(cctxv[...].astype(F32), (8, cctxv.shape[1]))).astype(BF16)
    half = samples // 2
    weights = modv[...].reshape(-1, modv.shape[2])
    rows = dot_t(act, weights)
    side = dot_t(act_c, weights[0:LANES])
    gates = jnp.concatenate([rows[:half, LANES:], rows[half:, LANES:]], axis=1)
    zsend[0:samples, :] = rows[:, 0:LANES].astype(BF16)
    zsend[8:16, :] = jnp.concatenate([side[0:8 - half], gates], axis=0).astype(BF16)

    def norm_rows(src, dst, rows):
        def step(i, _):
            r = pl.ds(pl.multiple_of(i * rows, rows), rows)
            v = src[r, :].astype(F32)
            v = v - jnp.mean(v, axis=-1, keepdims=True)
            dst[r, :] = v * lax.rsqrt(jnp.mean(v * v, axis=-1, keepdims=True) + EPS)
            return 0

        lax.fori_loop(0, src.shape[0] // rows, step, 0)

    loads[3].wait()
    norm_rows(xv, xn, REACH)

    pl.semaphore_wait(barrier, len(z_far) + len(xy_off))
    for d in z_far:
        pltpu.make_async_remote_copy(
            src_ref=zsend, dst_ref=zrecv.at[d - 1], send_sem=z_send, recv_sem=z_recv,
            device_id=z_at(d), device_id_type=MESH,
        ).start()

    loads[4].wait()
    norm_rows(cxv, cxn, C)
    kvc[:, LANES:] = jnp.ones((kvc.shape[0], LANES), BF16)
    kvx[:, LANES:] = jnp.ones((kvx.shape[0], LANES), BF16)

    lane = lane_iota((T, LANES))
    pos = lax.broadcasted_iota(jnp.int32, (T, LANES), 0) + sp * T
    inner = lane & 31
    freq = jnp.exp((inner & 15).astype(F32) * (-2.0 / 32.0 * math.log(BASE)))
    place = jnp.where((lane & 63) < 32, pos >> 6, pos & 63).astype(F32)
    angle = place * freq
    ct[...] = jnp.cos(angle)
    sine = jnp.sin(angle)
    st[...] = jnp.where(inner < 16, -sine, sine)
    loads[5].wait()
    loads[6].wait()

    pltpu.make_async_copy(zrecv, zrecv, z_recv).wait()
    total = zsend[...].astype(F32)
    for d in range(SP - 1):
        total = total + zrecv[d].astype(F32)
    first_gate = 8 + 8 - half
    for s in range(samples):
        row = first_gate + s % half
        xysend[s, 0:1, :] = total[s:s + 1]
        xysend[s, 1:2, :] = total[8:9]
        xysend[s, 2:3, :] = total[row:row + 1]
        xysend[s, 3:4, :] = total[row:row + 1]
    me = tp * DP + dp
    for t, d in sorted(xy_off, key=lambda o: -(min(o[0], TP - o[0]) + min(o[1], DP - o[1]) // 2)):
        target = lax.rem(dp + d, DP)
        pltpu.make_async_remote_copy(
            src_ref=xysend.at[target], dst_ref=xyrecv.at[me], send_sem=xy_send, recv_sem=xy_recv,
            device_id={"tp": lax.rem(tp + t, TP), "dp": target}, device_id_type=MESH,
        ).start()
    xyrecv[me] = xysend[dp]
    others = xyrecv.at[pl.ds(0, len(xy_off))]
    pltpu.make_async_copy(others, others, xy_recv).wait()
    chunks = vecs.shape[1]
    low4 = lane_iota((4, LANES)) < 64
    extra = jnp.where(lax.broadcasted_iota(jnp.int32, (4, LANES), 0) < 2, 1.0, 0.0)
    for k in range(chunks):
        left, right = xyrecv[2 * k], xyrecv[2 * k + 1]
        vecs[0, k] = jnp.where(low4, left, pltpu.roll(right, 64, 1))
        vecs[1, k] = jnp.where(low4, pltpu.roll(left, 64, 1), right) + extra

    def modulate(src, dst, row):
        def step(k, _):
            c = pl.ds(pl.multiple_of(k * LANES, LANES), LANES)
            shift = vecs[0, k, row:row + 1, :]
            scale = vecs[1, k, row:row + 1, :]
            dst[:, c] = (src[:, c] * scale + shift).astype(BF16)
            return 0

        lax.fori_loop(0, chunks, step, 0)

    def ctx_at(d, count=1):
        return kvc.at[pl.ds(SLOT[d] * C, count * C), pl.ds(0, LANES)]

    def ctx_copy(slot_from, slot_to, d, sem):
        return pltpu.make_async_remote_copy(
            src_ref=ctx_at(slot_from), dst_ref=ctx_at(slot_to), send_sem=c_send, recv_sem=c_recv.at[sem],
            device_id=z_at(d), device_id_type=MESH,
        )

    modulate(cxn, cxb, 1)
    kvc[0:C, 0:LANES] = dot_t(cxb[...], kvw[...]).astype(BF16)
    for d in DIRECT:
        ctx_copy(0, d, d, {5: 1, -5: 2}.get(d, 0)).start()

    modulate(xn, xb, 0)

    def partner(v):
        low = (lane_iota(v.shape) & 31) < 16
        return jnp.where(low, pltpu.roll(v, LANES - 16, 1), pltpu.roll(v, 16, 1))

    kv = dot_t(xb[...], kvw[...])
    is_key = lane_iota((T, LANES)) < 64
    kv = jnp.where(is_key, kv * ct[...] + partner(kv) * st[...], kv)
    kvx[REACH:REACH + T, 0:LANES] = kv.astype(BF16)
    sends = []
    for side_index, (at, to, there_at) in enumerate(((T, 1, 0), (REACH, -1, REACH + T))):
        copy = pltpu.make_async_remote_copy(
            src_ref=kvx.at[pl.ds(at, REACH), pl.ds(0, LANES)], dst_ref=kvx.at[pl.ds(there_at, REACH), pl.ds(0, LANES)],
            send_sem=h_send.at[side_index], recv_sem=h_recv.at[side_index], device_id=z_at(to), device_id_type=MESH,
        )
        copy.start()
        sends.append(copy)

    loads[7].wait()
    factor = LOG2E * HEAD ** (-0.5)
    low_lane = lane_iota((T, LANES)) < 64
    for j in range(width // LANES):
        q = dot(xb[...], qwv[:, j * LANES:(j + 1) * LANES])
        q = (q * ct[...] + partner(q) * st[...]) * factor
        qz[2 * j] = jnp.where(low_lane, q, 0.0).astype(BF16)
        qz[2 * j + 1] = jnp.where(low_lane, pltpu.roll(q, 64, 1), 0.0).astype(BF16)

    loads[9].wait()
    loads[10].wait()

    def per_head(ref):
        return jnp.concatenate([jnp.full((REACH, LANES), ref[h] * LOG2E, F32) for h in range(heads)], axis=0)

    def queries(b):
        return qz[:, b * REACH:(b + 1) * REACH, :].reshape(heads * REACH, LANES)

    def window(b):
        keys = kvx[b * REACH:(b + 3) * REACH, :]
        s = dot_t(queries(b), keys[:, 0:LANES])
        i = lax.broadcasted_iota(jnp.int32, (REACH, 3 * REACH), 0)
        j = lax.broadcasted_iota(jnp.int32, (REACH, 3 * REACH), 1)
        valid = (j >= i) & (j <= i + 2 * REACH)
        if b == 0:
            valid = valid & (sp * T - REACH + j >= 0)
        if b == blocks - 1:
            valid = valid & (sp * T + (b - 1) * REACH + j < SP * T)
        s = jnp.where(valid[None], s.reshape(heads, REACH, 3 * REACH), MASKED).reshape(heads * REACH, 3 * REACH)
        m = full(jnp.max(s, axis=1, keepdims=True))
        accw[b] = dot(jnp.exp2(s - wide(m, 3 * REACH)).astype(BF16), keys)
        mw[b] = m

    pltpu.make_async_copy(ctx_at(5), ctx_at(5), c_recv.at[1]).wait()
    for slot_to, d in ((8, 3), (7, 2), (6, 1), (3, -2), (4, -1)):
        ctx_copy(5, slot_to, d, 3).start()
    pltpu.make_async_copy(ctx_at(-5), ctx_at(-5), c_recv.at[2]).wait()
    for slot_to, d in ((-7, -2), (-6, -1), (-4, 1)):
        ctx_copy(-5, slot_to, d, 3).start()
    for copy in sends:
        copy.wait_recv()
    pltpu.make_async_copy(ctx_at(1, NEAR), ctx_at(1, NEAR), c_recv.at[0]).wait()

    first_keys = (1 + len(DIRECT)) * C

    def context(b, keys, others):
        s = dot_t(queries(b), keys[:, 0:LANES])
        bias2 = per_head(biass)
        m0 = mw[b]
        m = jnp.maximum(m0, full(jnp.max(s, axis=1, keepdims=True)) + bias2)
        if others is not None:
            m = jnp.maximum(m, others)
        p = jnp.exp2(s - wide(m - bias2, keys.shape[0])).astype(BF16)
        return m, dot(p, keys) + accw[b] * wide(jnp.exp2(m0 - m), 2 * LANES)

    for b in range(blocks):
        window(b)
    for b in range(blocks):
        m, acc = context(b, kvc[0:first_keys, :], None)
        accw[b] = acc
        mw[b] = m

    rest = ctx_at(RELAYED[0], len(RELAYED))
    pltpu.make_async_copy(rest, rest, c_recv.at[3]).wait()

    def tp_copy(b, way):
        up = way in (0, 2)
        owner = tp if way < 2 else lax.rem(tp + (TP - 1 if up else 1), TP)
        rows = pl.ds(b * REACH + (REACH // 2 if way == 3 else 0), REACH // 2 if way >= 2 else REACH)
        return pltpu.make_async_remote_copy(
            src_ref=gath.at[owner, rows], dst_ref=gath.at[owner, rows], send_sem=y_send.at[b, way],
            recv_sem=y_recv.at[b, way], device_id={"tp": lax.rem(tp + (1 if up else TP - 1), TP)}, device_id_type=MESH,
        )

    for b in range(blocks):
        sink2 = per_head(sinks)
        m, acc = context(b, kvc[first_keys:, :], sink2)
        att = acc[:, 0:LANES] / (acc[:, LANES:] + jnp.exp2(sink2 - m))
        att = att.reshape(heads, REACH, LANES)
        low = lane_iota((REACH, LANES)) < 64
        for j in range(heads // 2):
            pair = jnp.where(low, pltpu.roll(att[2 * j], 64, 1), att[2 * j + 1])
            gath[tp, b * REACH:(b + 1) * REACH, j * LANES:(j + 1) * LANES] = pair.astype(BF16)
        tp_copy(b, 0).start()
        tp_copy(b, 1).start()

    for b in range(blocks):
        for way in (0, 1):
            tp_copy(b, way).wait_recv()
            tp_copy(b, way + 2).start()

    loads[8].wait()
    gate_rows = [tp * (cols // LANES) + j for j in range(cols // LANES)]
    gate = jnp.concatenate(
        [jnp.where(dp < half, vecs[0, k, 2:3, :], vecs[1, k, 2:3, :]) for k in gate_rows], axis=1
    )

    for b in range(blocks):
        rows = pl.ds(b * REACH, REACH)
        tp_copy(b, 2).wait_recv()
        tp_copy(b, 3).wait_recv()
        mixed = dot(gath[0, rows, :], owv[0:width, :])
        for t in range(1, TP):
            mixed = mixed + dot(gath[t, rows, :], owv[t * width:(t + 1) * width, :])
        own = xv[rows, pl.ds(pl.multiple_of(tp * cols, LANES), cols)].astype(F32)
        outv[rows, :] = own + gate * mixed
        pltpu.make_async_copy(outv.at[rows], out.at[rows], out_sem.at[b]).start()

    for b in range(blocks):
        pltpu.make_async_copy(outv.at[pl.ds(b * REACH, REACH)], out.at[pl.ds(b * REACH, REACH)], out_sem.at[b]).wait()
        for way in range(4):
            tp_copy(b, way).wait_send()
    for copy in sends:
        copy.wait_send()
    pltpu.make_async_copy(zrecv, zrecv, z_send).wait()
    others = xyrecv.at[pl.ds(0, len(xy_off))]
    pltpu.make_async_copy(others, others, xy_send).wait()
    others = kvc.at[pl.ds(C, (SP - 1) * C), pl.ds(0, LANES)]
    pltpu.make_async_copy(others, others, c_send).wait()


def per_device(sizes, lat, cond, cctx, mod, ctx, qw, kw, vw, ow, sink, bias):
    SP, TP, DP = sizes
    T, D = lat.shape[1:]
    C = ctx.shape[1]
    width = qw.shape[1]
    heads = width // HEAD
    blocks = T // REACH
    cols = ow.shape[1]
    samples = cond.shape[0]
    any_space = pl.BlockSpec(memory_space=pl.ANY)
    vmem = pltpu.VMEM
    dma = pltpu.SemaphoreType.DMA
    scratch = [
        vmem((T, D), BF16), vmem(cond.shape, BF16), vmem((1, cctx.shape[0]), BF16), vmem((mod.shape[0], mod.shape[2], mod.shape[1]), BF16),
        vmem((C, D), BF16), vmem(qw.shape, BF16), vmem(ow.shape, BF16),
        pltpu.SMEM(sink.shape, F32), pltpu.SMEM(bias.shape, F32),
        vmem((16, LANES), BF16), vmem((SP - 1, 16, LANES), BF16),
        vmem((samples, 4, LANES), F32), vmem((TP * DP, 4, LANES), F32), vmem((2, TP * DP // 2, 4, LANES), F32),
        vmem((T, D), F32), vmem((C, D), F32), vmem((T, D), BF16), vmem((C, D), BF16), vmem((LANES, D), BF16),
        vmem((T, LANES), F32), vmem((T, LANES), F32),
        vmem((SP * C, 2 * LANES), BF16), vmem((T + 2 * REACH, 2 * LANES), BF16), vmem((heads, T, LANES), BF16),
        vmem((blocks, heads * REACH, 2 * LANES), F32), vmem((blocks, heads * REACH, LANES), F32),
        vmem((TP, T, width), BF16), vmem((T, cols), F32),
        dma((11,)), dma((blocks,)),
        dma, dma, dma, dma, dma, dma((4,)), dma((2,)), dma((2,)), dma((blocks, 4)), dma((blocks, 4)),
    ]
    result = pl.pallas_call(
        functools.partial(kernel, sizes),
        out_shape=jax.ShapeDtypeStruct((T, cols), F32),
        in_specs=[any_space] * 11,
        out_specs=any_space,
        scratch_shapes=scratch,
        compiler_params=pltpu.CompilerParams(
            collective_id=0, has_side_effects=True, vmem_limit_bytes=60 * 1024 * 1024
        ),
        name="step",
    )(lat[0], cond, cctx[None, :], mod.transpose(0, 2, 1), ctx[0], qw, kw.T, vw.T, ow, sink, bias)
    return result[None]


def solution(mesh):
    placed = (
        P("dp", "sp", None),
        P(None, "sp"),
        P("sp"),
        P(None, "sp", ("tp", "dp")),
        P("dp", "sp", None),
        P(None, "tp"),
        P(None, "tp"),
        P(None, "tp"),
        P(None, "tp"),
        P("tp"),
        P("tp"),
    )
    sizes = (mesh.shape["sp"], mesh.shape["tp"], mesh.shape["dp"])
    return jax.shard_map(
        functools.partial(per_device, sizes),
        mesh=mesh, in_specs=placed, out_specs=P("dp", "sp", "tp"), check_vma=False,
    )
```

time: 68.2 us -> 52.5 us (0.77)
  the two profiles are of different devices: /device:TPU:1 before, /device:TPU:32 now
where the time goes in v2:
time: 52.5 us; the launch traced here: 52.3 us
  Pallas kernels  50.3 us (96%)
  local copies, waits for them, and re-layouts  2.06 us (4%)
    pallas_call x1, Pallas kernels, per_device(): pl.pallas_call(functools.partial(kernel, sizes), out_shape=jax.ShapeDtype...  50.3 us
    unnamed x1, local copies, waits for them, and re-layouts  2.06 us

profile of v2, /device:TPU:32, one launch (start us, length us, event | category | flops | bytes accessed | tf_op | source)
XLA Modules:
  0.0 52.3 jit_solution(6484170793431852973)
XLA Ops:
  0.0 50.3 %step.1 = f32[384,512]{1,0:T(8,128)} custom-call(bf16[384,2048]{1,0:T(8,128)(2,1)} %bitcast.8, bf16[8,128]{1,0:T(8,128)(2,1)} %cond.1, bf16[1,128]{1,0:T(2,128)(2,1)} %bitcast.13, bf16[3,64,128]{2,1,0:T(8,128)(2,1)} %bitcast.12, bf16[64,2048]{1,0:T(8,128)(2,1)} %bitcast.9, bf16[2048,256]{1,0:T(8,128)(2,1)} %qw.1, bf16[64,2048]{1,0:T(8,128)(2,1)} %bitcast.10, ...), custom_call_target="tpu_custom_call" | custom-call | tf_op jit(solution)/shard_map/step/pallas_call | solution.py:361
  50.3 2.1 %copy.13 = f32[1,384,512]{2,1,0:T(8,128)} copy(f32[1,384,512]{2,1,0:T(8,128)} %bitcast.7) | data formatting | bytes 1572864

commit v3 on v2

--- a/solution.py
+++ b/solution.py
@@ -42,9 +42,11 @@
 
 
 DIRECT = (5, -5, 1, -1, 2, -2, -3)
-RELAYED = (3, 4, 6, 7, 8, -4, -6, -7)
-SLOT = {0: 0, **{d: i + 1 for i, d in enumerate((1, -1, 2, -2, -3, 5, -5) + RELAYED)}}
-NEAR = 5
+NEAR = (1, -1, 2, -2, -3)
+SOON = (4, 6, -4, -6)
+LATE = (3, 7, 8, -7)
+SLOT = {d: i for i, d in enumerate((0, *NEAR, 5, -5, *SOON, *LATE))}
+PIECE = 128
 
 
 def kernel(
@@ -54,8 +56,8 @@
     xv, condv, cctxv, modv, cxv, qwv, owv, sinks, biass,
     zsend, zrecv, xysend, xyrecv, vecs,
     xn, cxn, xb, cxb, kvw, ct, st,
-    kvc, kvx, qz, accw, mw, gath, outv,
-    in_sems, out_sem,
+    kvc, kvx, qz, accw, mw, gath,
+    in_sems,
     z_send, z_recv, xy_send, xy_recv, c_send, c_recv, h_send, h_recv, y_send, y_recv,
 ):
     SP, TP, DP = sizes
@@ -168,16 +170,6 @@
         vecs[0, k] = jnp.where(low4, left, pltpu.roll(right, 64, 1))
         vecs[1, k] = jnp.where(low4, pltpu.roll(left, 64, 1), right) + extra
 
-    def modulate(src, dst, row):
-        def step(k, _):
-            c = pl.ds(pl.multiple_of(k * LANES, LANES), LANES)
-            shift = vecs[0, k, row:row + 1, :]
-            scale = vecs[1, k, row:row + 1, :]
-            dst[:, c] = (src[:, c] * scale + shift).astype(BF16)
-            return 0
-
-        lax.fori_loop(0, chunks, step, 0)
-
     def ctx_at(d, count=1):
         return kvc.at[pl.ds(SLOT[d] * C, count * C), pl.ds(0, LANES)]
 
@@ -187,12 +179,19 @@
             device_id=z_at(d), device_id_type=MESH,
         )
 
-    modulate(cxn, cxb, 1)
+    for k in range(chunks):
+        c = slice(k * LANES, (k + 1) * LANES)
+        cxb[:, c] = (cxn[:, c] * vecs[1, k, 1:2, :] + vecs[0, k, 1:2, :]).astype(BF16)
     kvc[0:C, 0:LANES] = dot_t(cxb[...], kvw[...]).astype(BF16)
     for d in DIRECT:
         ctx_copy(0, d, d, {5: 1, -5: 2}.get(d, 0)).start()
 
-    modulate(xn, xb, 0)
+    def modulate(k, _):
+        c = pl.ds(pl.multiple_of(k * LANES, LANES), LANES)
+        xb[:, c] = (xn[:, c] * vecs[1, k, 0:1, :] + vecs[0, k, 0:1, :]).astype(BF16)
+        return 0
+
+    lax.fori_loop(0, chunks, modulate, 0)
 
     def partner(v):
         low = (lane_iota(v.shape) & 31) < 16
@@ -223,15 +222,19 @@
     loads[9].wait()
     loads[10].wait()
 
-    def per_head(ref):
-        return jnp.concatenate([jnp.full((REACH, LANES), ref[h] * LOG2E, F32) for h in range(heads)], axis=0)
-
-    def queries(b):
-        return qz[:, b * REACH:(b + 1) * REACH, :].reshape(heads * REACH, LANES)
+    def per_head(ref, count):
+        return jnp.concatenate([jnp.full((count, LANES), ref[h] * LOG2E, F32) for h in range(heads)], axis=0)
+
+    def of_rows(ref, start, count):
+        return ref[:, start:start + count, :].reshape(heads * count, ref.shape[2])
+
+    def keep_state(start, count, m, acc):
+        mw[:, start:start + count, :] = m.reshape(heads, count, LANES)
+        accw[:, start:start + count, :] = acc.reshape(heads, count, 2 * LANES)
 
     def window(b):
         keys = kvx[b * REACH:(b + 3) * REACH, :]
-        s = dot_t(queries(b), keys[:, 0:LANES])
+        s = dot_t(of_rows(qz, b * REACH, REACH), keys[:, 0:LANES])
         i = lax.broadcasted_iota(jnp.int32, (REACH, 3 * REACH), 0)
         j = lax.broadcasted_iota(jnp.int32, (REACH, 3 * REACH), 1)
         valid = (j >= i) & (j <= i + 2 * REACH)
@@ -241,66 +244,70 @@
             valid = valid & (sp * T + (b - 1) * REACH + j < SP * T)
         s = jnp.where(valid[None], s.reshape(heads, REACH, 3 * REACH), MASKED).reshape(heads * REACH, 3 * REACH)
         m = full(jnp.max(s, axis=1, keepdims=True))
-        accw[b] = dot(jnp.exp2(s - wide(m, 3 * REACH)).astype(BF16), keys)
-        mw[b] = m
-
-    pltpu.make_async_copy(ctx_at(5), ctx_at(5), c_recv.at[1]).wait()
-    for slot_to, d in ((8, 3), (7, 2), (6, 1), (3, -2), (4, -1)):
-        ctx_copy(5, slot_to, d, 3).start()
-    pltpu.make_async_copy(ctx_at(-5), ctx_at(-5), c_recv.at[2]).wait()
-    for slot_to, d in ((-7, -2), (-6, -1), (-4, 1)):
-        ctx_copy(-5, slot_to, d, 3).start()
-    for copy in sends:
-        copy.wait_recv()
-    pltpu.make_async_copy(ctx_at(1, NEAR), ctx_at(1, NEAR), c_recv.at[0]).wait()
-
-    first_keys = (1 + len(DIRECT)) * C
-
-    def context(b, keys, others):
-        s = dot_t(queries(b), keys[:, 0:LANES])
-        bias2 = per_head(biass)
-        m0 = mw[b]
+        keep_state(b * REACH, REACH, m, dot(jnp.exp2(s - wide(m, 3 * REACH)).astype(BF16), keys))
+
+    def arrived(d, count, sem):
+        blocks_here = ctx_at(d, count)
+        pltpu.make_async_copy(blocks_here, blocks_here, c_recv.at[sem]).wait()
+
+    def context(start, count, keys, others):
+        s = dot_t(of_rows(qz, start, count), keys[:, 0:LANES])
+        bias2 = per_head(biass, count)
+        m0 = of_rows(mw, start, count)
         m = jnp.maximum(m0, full(jnp.max(s, axis=1, keepdims=True)) + bias2)
         if others is not None:
             m = jnp.maximum(m, others)
         p = jnp.exp2(s - wide(m - bias2, keys.shape[0])).astype(BF16)
-        return m, dot(p, keys) + accw[b] * wide(jnp.exp2(m0 - m), 2 * LANES)
-
-    for b in range(blocks):
+        return m, dot(p, keys) + of_rows(accw, start, count) * wide(jnp.exp2(m0 - m), 2 * LANES)
+
+    soon, late = SLOT[SOON[0]] * C, SLOT[LATE[0]] * C
+
+    for b in range(1, blocks - 1):
+        window(b)
+    arrived(5, 1, 1)
+    for slot_to, d in ((8, 3), (7, 2), (3, -2), (6, 1), (4, -1)):
+        ctx_copy(5, slot_to, d, 4 if slot_to in LATE else 3).start()
+    arrived(-5, 1, 2)
+    for slot_to, d in ((-7, -2), (-6, -1), (-4, 1)):
+        ctx_copy(-5, slot_to, d, 4 if slot_to in LATE else 3).start()
+    for copy in sends:
+        copy.wait_recv()
+    arrived(NEAR[0], len(NEAR), 0)
+    for b in (0, blocks - 1):
         window(b)
     for b in range(blocks):
-        m, acc = context(b, kvc[0:first_keys, :], None)
-        accw[b] = acc
-        mw[b] = m
-
-    rest = ctx_at(RELAYED[0], len(RELAYED))
-    pltpu.make_async_copy(rest, rest, c_recv.at[3]).wait()
-
-    def tp_copy(b, way):
+        keep_state(b * REACH, REACH, *context(b * REACH, REACH, kvc[0:soon, :], None))
+    arrived(SOON[0], len(SOON), 3)
+    for b in range(blocks):
+        keep_state(b * REACH, REACH, *context(b * REACH, REACH, kvc[soon:late, :], None))
+    arrived(LATE[0], len(LATE), 4)
+
+    def tp_copy(i, way):
         up = way in (0, 2)
         owner = tp if way < 2 else lax.rem(tp + (TP - 1 if up else 1), TP)
-        rows = pl.ds(b * REACH + (REACH // 2 if way == 3 else 0), REACH // 2 if way >= 2 else REACH)
+        rows = pl.ds(i * PIECE + (PIECE // 2 if way == 3 else 0), PIECE // 2 if way >= 2 else PIECE)
         return pltpu.make_async_remote_copy(
-            src_ref=gath.at[owner, rows], dst_ref=gath.at[owner, rows], send_sem=y_send.at[b, way],
-            recv_sem=y_recv.at[b, way], device_id={"tp": lax.rem(tp + (1 if up else TP - 1), TP)}, device_id_type=MESH,
+            src_ref=gath.at[owner, rows], dst_ref=gath.at[owner, rows], send_sem=y_send.at[i, way],
+            recv_sem=y_recv.at[i, way], device_id={"tp": lax.rem(tp + (1 if up else TP - 1), TP)}, device_id_type=MESH,
         )
 
-    for b in range(blocks):
-        sink2 = per_head(sinks)
-        m, acc = context(b, kvc[first_keys:, :], sink2)
+    pieces = T // PIECE
+    sink2 = per_head(sinks, PIECE)
+    low = lane_iota((PIECE, LANES)) < 64
+    for i in range(pieces):
+        m, acc = context(i * PIECE, PIECE, kvc[late:, :], sink2)
         att = acc[:, 0:LANES] / (acc[:, LANES:] + jnp.exp2(sink2 - m))
-        att = att.reshape(heads, REACH, LANES)
-        low = lane_iota((REACH, LANES)) < 64
+        att = att.reshape(heads, PIECE, LANES)
         for j in range(heads // 2):
             pair = jnp.where(low, pltpu.roll(att[2 * j], 64, 1), att[2 * j + 1])
-            gath[tp, b * REACH:(b + 1) * REACH, j * LANES:(j + 1) * LANES] = pair.astype(BF16)
-        tp_copy(b, 0).start()
-        tp_copy(b, 1).start()
-
-    for b in range(blocks):
+            gath[tp, i * PIECE:(i + 1) * PIECE, j * LANES:(j + 1) * LANES] = pair.astype(BF16)
+        tp_copy(i, 0).start()
+        tp_copy(i, 1).start()
+
+    for i in range(pieces):
         for way in (0, 1):
-            tp_copy(b, way).wait_recv()
-            tp_copy(b, way + 2).start()
+            tp_copy(i, way).wait_recv()
+            tp_copy(i, way + 2).start()
 
     loads[8].wait()
     gate_rows = [tp * (cols // LANES) + j for j in range(cols // LANES)]
@@ -310,19 +317,18 @@
 
     for b in range(blocks):
         rows = pl.ds(b * REACH, REACH)
-        tp_copy(b, 2).wait_recv()
-        tp_copy(b, 3).wait_recv()
+        for i in range(b * REACH // PIECE, (b + 1) * REACH // PIECE):
+            tp_copy(i, 2).wait_recv()
+            tp_copy(i, 3).wait_recv()
         mixed = dot(gath[0, rows, :], owv[0:width, :])
         for t in range(1, TP):
             mixed = mixed + dot(gath[t, rows, :], owv[t * width:(t + 1) * width, :])
         own = xv[rows, pl.ds(pl.multiple_of(tp * cols, LANES), cols)].astype(F32)
-        outv[rows, :] = own + gate * mixed
-        pltpu.make_async_copy(outv.at[rows], out.at[rows], out_sem.at[b]).start()
-
-    for b in range(blocks):
-        pltpu.make_async_copy(outv.at[pl.ds(b * REACH, REACH)], out.at[pl.ds(b * REACH, REACH)], out_sem.at[b]).wait()
+        out[rows, :] = own + gate * mixed
+
+    for i in range(pieces):
         for way in range(4):
-            tp_copy(b, way).wait_send()
+            tp_copy(i, way).wait_send()
     for copy in sends:
         copy.wait_send()
     pltpu.make_async_copy(zrecv, zrecv, z_send).wait()
@@ -353,22 +359,24 @@
         vmem((T, D), F32), vmem((C, D), F32), vmem((T, D), BF16), vmem((C, D), BF16), vmem((LANES, D), BF16),
         vmem((T, LANES), F32), vmem((T, LANES), F32),
         vmem((SP * C, 2 * LANES), BF16), vmem((T + 2 * REACH, 2 * LANES), BF16), vmem((heads, T, LANES), BF16),
-        vmem((blocks, heads * REACH, 2 * LANES), F32), vmem((blocks, heads * REACH, LANES), F32),
-        vmem((TP, T, width), BF16), vmem((T, cols), F32),
-        dma((11,)), dma((blocks,)),
-        dma, dma, dma, dma, dma, dma((4,)), dma((2,)), dma((2,)), dma((blocks, 4)), dma((blocks, 4)),
+        vmem((heads, T, 2 * LANES), F32), vmem((heads, T, LANES), F32),
+        vmem((TP, T, width), BF16),
+        dma((11,)),
+        dma, dma, dma, dma, dma, dma((5,)), dma((2,)), dma((2,)), dma((T // PIECE, 4)), dma((T // PIECE, 4)),
     ]
     result = pl.pallas_call(
         functools.partial(kernel, sizes),
-        out_shape=jax.ShapeDtypeStruct((T, cols), F32),
+        out_shape=vmem((T, cols), F32),
         in_specs=[any_space] * 11,
-        out_specs=any_space,
+        out_specs=pl.BlockSpec(memory_space=vmem),
         scratch_shapes=scratch,
         compiler_params=pltpu.CompilerParams(
-            collective_id=0, has_side_effects=True, vmem_limit_bytes=60 * 1024 * 1024
+            collective_id=0, has_side_effects=True, vmem_limit_bytes=48 * 1024 * 1024
         ),
         name="step",
-    )(lat[0], cond, cctx[None, :], mod.transpose(0, 2, 1), ctx[0], qw, kw.T, vw.T, ow, sink, bias)
+    )(*(pltpu.with_memory_space_constraint(v, pltpu.HBM) for v in (
+        lat[0], cond, cctx[None, :], mod.transpose(0, 2, 1), ctx[0], qw, kw.T, vw.T, ow, sink, bias
+    )))
     return result[None]
 
 

time: 52.5 us -> 50.6 us (0.964)
  the two profiles are of different devices: /device:TPU:32 before, /device:TPU:16 now
where the time goes in v3:
time: 50.6 us; the launch traced here: 50.5 us
  Pallas kernels  49.6 us (98%)
  local copies, waits for them, and re-layouts  0.88 us (2%)
    pallas_call x1, Pallas kernels, per_device(): pl.pallas_call(functools.partial(kernel, sizes), out_shape=vmem((T, cols)...  49.6 us

profile of v3, /device:TPU:16, one launch (start us, length us, event | category | flops | bytes accessed | tf_op | source)
XLA Modules:
  0.0 50.5 jit_solution(1834822665290120274)
XLA Ops:
  0.0 49.6 %step.1 = f32[384,512]{1,0:T(8,128)S(1)} custom-call(bf16[384,2048]{1,0:T(8,128)(2,1)} %bitcast.8, bf16[8,128]{1,0:T(8,128)(2,1)} %cond.1, bf16[1,128]{1,0:T(2,128)(2,1)} %bitcast.13, bf16[3,64,128]{2,1,0:T(8,128)(2,1)} %bitcast.12, bf16[64,2048]{1,0:T(8,128)(2,1)} %bitcast.9, bf16[2048,256]{1,0:T(8,128)(2,1)} %qw.1, bf16[64,2048]{1,0:T(8,128)(2,1)} %bitcast.10, ...), custom_call_target="tpu_custom_call" | custom-call | tf_op jit(solution)/shard_map/step/pallas_call | solution.py:367
  49.6 0.9 %copy.13 = f32[1,384,512]{2,1,0:T(8,128)} copy(f32[1,384,512]{2,1,0:T(8,128)S(1)} %bitcast.7) | data formatting | bytes 1572864

commit v4 on v3

--- a/solution.py
+++ b/solution.py
@@ -46,7 +46,8 @@
 SOON = (4, 6, -4, -6)
 LATE = (3, 7, 8, -7)
 SLOT = {d: i for i, d in enumerate((0, *NEAR, 5, -5, *SOON, *LATE))}
-PIECE = 128
+PIECE = 64
+Z_ROWS = 10
 
 
 def kernel(
@@ -54,11 +55,11 @@
     lat, cond, cctx, mod, ctx, qw, kw, vw, ow, sink, bias,
     out,
     xv, condv, cctxv, modv, cxv, qwv, owv, sinks, biass,
-    zsend, zrecv, xysend, xyrecv, vecs,
+    zsend, zrecv, gsend, grecv, gsum, ghave, xysend, xyrecv, vecs,
     xn, cxn, xb, cxb, kvw, ct, st,
-    kvc, kvx, qz, accw, mw, gath,
+    kvc, kvx, qz, accw, mw, gath, mixed,
     in_sems,
-    z_send, z_recv, xy_send, xy_recv, c_send, c_recv, h_send, h_recv, y_send, y_recv,
+    z_send, z_recv, xy_send, xy_recv, c_send, c_recv, h_send, h_recv, y_send, y_recv, g_sems,
 ):
     SP, TP, DP = sizes
     T, D = xv.shape
@@ -100,9 +101,9 @@
     weights = modv[...].reshape(-1, modv.shape[2])
     rows = dot_t(act, weights)
     side = dot_t(act_c, weights[0:LANES])
-    gates = jnp.concatenate([rows[:half, LANES:], rows[half:, LANES:]], axis=1)
     zsend[0:samples, :] = rows[:, 0:LANES].astype(BF16)
-    zsend[8:16, :] = jnp.concatenate([side[0:8 - half], gates], axis=0).astype(BF16)
+    zsend[samples:, :] = side[0:Z_ROWS - samples].astype(BF16)
+    gsend[...] = jnp.concatenate([rows[:half, LANES:], rows[half:, LANES:]], axis=1)
 
     def norm_rows(src, dst, rows):
         def step(i, _):
@@ -114,9 +115,6 @@
 
         lax.fori_loop(0, src.shape[0] // rows, step, 0)
 
-    loads[3].wait()
-    norm_rows(xv, xn, REACH)
-
     pl.semaphore_wait(barrier, len(z_far) + len(xy_off))
     for d in z_far:
         pltpu.make_async_remote_copy(
@@ -124,6 +122,8 @@
             device_id=z_at(d), device_id_type=MESH,
         ).start()
 
+    loads[3].wait()
+    norm_rows(xv, xn, REACH)
     loads[4].wait()
     norm_rows(cxv, cxn, C)
     kvc[:, LANES:] = jnp.ones((kvc.shape[0], LANES), BF16)
@@ -145,13 +145,9 @@
     total = zsend[...].astype(F32)
     for d in range(SP - 1):
         total = total + zrecv[d].astype(F32)
-    first_gate = 8 + 8 - half
     for s in range(samples):
-        row = first_gate + s % half
         xysend[s, 0:1, :] = total[s:s + 1]
-        xysend[s, 1:2, :] = total[8:9]
-        xysend[s, 2:3, :] = total[row:row + 1]
-        xysend[s, 3:4, :] = total[row:row + 1]
+        xysend[s, 1:2, :] = total[samples:samples + 1]
     me = tp * DP + dp
     for t, d in sorted(xy_off, key=lambda o: -(min(o[0], TP - o[0]) + min(o[1], DP - o[1]) // 2)):
         target = lax.rem(dp + d, DP)
@@ -160,15 +156,19 @@
             device_id={"tp": lax.rem(tp + t, TP), "dp": target}, device_id_type=MESH,
         ).start()
     xyrecv[me] = xysend[dp]
+    for d in z_far:
+        pltpu.make_async_remote_copy(
+            src_ref=gsend, dst_ref=grecv.at[d - 1], send_sem=g_sems.at[0], recv_sem=g_sems.at[1],
+            device_id=z_at(d), device_id_type=MESH,
+        ).start()
     others = xyrecv.at[pl.ds(0, len(xy_off))]
     pltpu.make_async_copy(others, others, xy_recv).wait()
     chunks = vecs.shape[1]
-    low4 = lane_iota((4, LANES)) < 64
-    extra = jnp.where(lax.broadcasted_iota(jnp.int32, (4, LANES), 0) < 2, 1.0, 0.0)
+    low2 = lane_iota((2, LANES)) < 64
     for k in range(chunks):
         left, right = xyrecv[2 * k], xyrecv[2 * k + 1]
-        vecs[0, k] = jnp.where(low4, left, pltpu.roll(right, 64, 1))
-        vecs[1, k] = jnp.where(low4, pltpu.roll(left, 64, 1), right) + extra
+        vecs[0, k] = jnp.where(low2, left, pltpu.roll(right, 64, 1))
+        vecs[1, k] = jnp.where(low2, pltpu.roll(left, 64, 1), right) + 1.0
 
     def ctx_at(d, count=1):
         return kvc.at[pl.ds(SLOT[d] * C, count * C), pl.ds(0, LANES)]
@@ -205,7 +205,7 @@
     for side_index, (at, to, there_at) in enumerate(((T, 1, 0), (REACH, -1, REACH + T))):
         copy = pltpu.make_async_remote_copy(
             src_ref=kvx.at[pl.ds(at, REACH), pl.ds(0, LANES)], dst_ref=kvx.at[pl.ds(there_at, REACH), pl.ds(0, LANES)],
-            send_sem=h_send.at[side_index], recv_sem=h_recv.at[side_index], device_id=z_at(to), device_id_type=MESH,
+            send_sem=h_send, recv_sem=h_recv.at[side_index], device_id=z_at(to), device_id_type=MESH,
         )
         copy.start()
         sends.append(copy)
@@ -262,6 +262,17 @@
 
     soon, late = SLOT[SOON[0]] * C, SLOT[LATE[0]] * C
 
+    pltpu.make_async_copy(grecv, grecv, g_sems.at[1]).wait()
+    gates = gsend[...]
+    for d in range(SP - 1):
+        gates = gates + grecv[d]
+    gsum[...] = gates
+    ghave[dp] = gates
+    for d in range(1, DP):
+        pltpu.make_async_remote_copy(
+            src_ref=gsum, dst_ref=ghave.at[dp], send_sem=g_sems.at[2], recv_sem=g_sems.at[3],
+            device_id={"dp": lax.rem(dp + d, DP)}, device_id_type=MESH,
+        ).start()
     for b in range(1, blocks - 1):
         window(b)
     arrived(5, 1, 1)
@@ -287,51 +298,67 @@
         owner = tp if way < 2 else lax.rem(tp + (TP - 1 if up else 1), TP)
         rows = pl.ds(i * PIECE + (PIECE // 2 if way == 3 else 0), PIECE // 2 if way >= 2 else PIECE)
         return pltpu.make_async_remote_copy(
-            src_ref=gath.at[owner, rows], dst_ref=gath.at[owner, rows], send_sem=y_send.at[i, way],
+            src_ref=gath.at[owner, rows], dst_ref=gath.at[owner, rows], send_sem=y_send,
             recv_sem=y_recv.at[i, way], device_id={"tp": lax.rem(tp + (1 if up else TP - 1), TP)}, device_id_type=MESH,
         )
 
     pieces = T // PIECE
-    sink2 = per_head(sinks, PIECE)
-    low = lane_iota((PIECE, LANES)) < 64
-    for i in range(pieces):
-        m, acc = context(i * PIECE, PIECE, kvc[late:, :], sink2)
+    sink2 = per_head(sinks, REACH)
+    low = lane_iota((REACH, LANES)) < 64
+    for b in range(blocks):
+        m, acc = context(b * REACH, REACH, kvc[late:, :], sink2)
         att = acc[:, 0:LANES] / (acc[:, LANES:] + jnp.exp2(sink2 - m))
-        att = att.reshape(heads, PIECE, LANES)
+        att = att.reshape(heads, REACH, LANES)
         for j in range(heads // 2):
             pair = jnp.where(low, pltpu.roll(att[2 * j], 64, 1), att[2 * j + 1])
-            gath[tp, i * PIECE:(i + 1) * PIECE, j * LANES:(j + 1) * LANES] = pair.astype(BF16)
-        tp_copy(i, 0).start()
-        tp_copy(i, 1).start()
-
-    for i in range(pieces):
-        for way in (0, 1):
-            tp_copy(i, way).wait_recv()
-            tp_copy(i, way + 2).start()
+            gath[tp, b * REACH:(b + 1) * REACH, j * LANES:(j + 1) * LANES] = pair.astype(BF16)
+        for i in range(b * REACH // PIECE, (b + 1) * REACH // PIECE):
+            tp_copy(i, 0).start()
+            tp_copy(i, 1).start()
 
     loads[8].wait()
-    gate_rows = [tp * (cols // LANES) + j for j in range(cols // LANES)]
-    gate = jnp.concatenate(
-        [jnp.where(dp < half, vecs[0, k, 2:3, :], vecs[1, k, 2:3, :]) for k in gate_rows], axis=1
-    )
-
+
+    def projected(owner, rows):
+        return dot(gath[owner, rows, :], owv[pl.ds(pl.multiple_of(owner * width, width), width), :])
+
+    above, below, opposite = (lax.rem(tp + t, TP) for t in (1, TP - 1, 2))
+    mixed[...] = projected(tp, pl.ds(0, T))
+    for b in range(blocks):
+        for i in range(b * REACH // PIECE, (b + 1) * REACH // PIECE):
+            for way in (0, 1):
+                tp_copy(i, way).wait_recv()
+                tp_copy(i, way + 2).start()
+        rows = pl.ds(b * REACH, REACH)
+        mixed[rows, :] = mixed[rows, :] + projected(above, rows) + projected(below, rows)
+
+    others = ghave.at[pl.ds(0, DP - 1)]
+    pltpu.make_async_copy(others, others, g_sems.at[3]).wait()
+    low1 = lane_iota((1, LANES)) < 64
+    gate_chunks = []
+    for k in range(DP // 2):
+        left, right = (ghave[2 * k + i, pl.ds(lax.rem(dp, half), 1), :] for i in range(2))
+        gate_chunks.append(jnp.where(
+            dp < half,
+            jnp.where(low1, left, pltpu.roll(right, 64, 1)),
+            jnp.where(low1, pltpu.roll(left, 64, 1), right),
+        ))
+    gate = jnp.concatenate(gate_chunks, axis=1)
     for b in range(blocks):
         rows = pl.ds(b * REACH, REACH)
         for i in range(b * REACH // PIECE, (b + 1) * REACH // PIECE):
             tp_copy(i, 2).wait_recv()
             tp_copy(i, 3).wait_recv()
-        mixed = dot(gath[0, rows, :], owv[0:width, :])
-        for t in range(1, TP):
-            mixed = mixed + dot(gath[t, rows, :], owv[t * width:(t + 1) * width, :])
         own = xv[rows, pl.ds(pl.multiple_of(tp * cols, LANES), cols)].astype(F32)
-        out[rows, :] = own + gate * mixed
-
-    for i in range(pieces):
-        for way in range(4):
-            tp_copy(i, way).wait_send()
-    for copy in sends:
-        copy.wait_send()
+        out[rows, :] = own + gate * (mixed[rows, :] + projected(opposite, rows))
+
+    others = gath.at[pl.ds(0, TP - 1)]
+    pltpu.make_async_copy(others, others, y_send).wait()
+    others = kvx.at[pl.ds(0, 2 * REACH), pl.ds(0, LANES)]
+    pltpu.make_async_copy(others, others, h_send).wait()
     pltpu.make_async_copy(zrecv, zrecv, z_send).wait()
+    pltpu.make_async_copy(grecv, grecv, g_sems.at[0]).wait()
+    others = ghave.at[pl.ds(0, DP - 1)]
+    pltpu.make_async_copy(others, others, g_sems.at[2]).wait()
     others = xyrecv.at[pl.ds(0, len(xy_off))]
     pltpu.make_async_copy(others, others, xy_send).wait()
     others = kvc.at[pl.ds(C, (SP - 1) * C), pl.ds(0, LANES)]
@@ -354,15 +381,17 @@
         vmem((T, D), BF16), vmem(cond.shape, BF16), vmem((1, cctx.shape[0]), BF16), vmem((mod.shape[0], mod.shape[2], mod.shape[1]), BF16),
         vmem((C, D), BF16), vmem(qw.shape, BF16), vmem(ow.shape, BF16),
         pltpu.SMEM(sink.shape, F32), pltpu.SMEM(bias.shape, F32),
-        vmem((16, LANES), BF16), vmem((SP - 1, 16, LANES), BF16),
-        vmem((samples, 4, LANES), F32), vmem((TP * DP, 4, LANES), F32), vmem((2, TP * DP // 2, 4, LANES), F32),
+        vmem((Z_ROWS, LANES), BF16), vmem((SP - 1, Z_ROWS, LANES), BF16),
+        vmem((samples // 2, LANES), F32), vmem((SP - 1, samples // 2, LANES), F32), vmem((samples // 2, LANES), F32),
+        vmem((DP, samples // 2, LANES), F32),
+        vmem((samples, 2, LANES), F32), vmem((TP * DP, 2, LANES), F32), vmem((2, TP * DP // 2, 2, LANES), F32),
         vmem((T, D), F32), vmem((C, D), F32), vmem((T, D), BF16), vmem((C, D), BF16), vmem((LANES, D), BF16),
         vmem((T, LANES), F32), vmem((T, LANES), F32),
         vmem((SP * C, 2 * LANES), BF16), vmem((T + 2 * REACH, 2 * LANES), BF16), vmem((heads, T, LANES), BF16),
         vmem((heads, T, 2 * LANES), F32), vmem((heads, T, LANES), F32),
-        vmem((TP, T, width), BF16),
+        vmem((TP, T, width), BF16), vmem((T, cols), F32),
         dma((11,)),
-        dma, dma, dma, dma, dma, dma((5,)), dma((2,)), dma((2,)), dma((T // PIECE, 4)), dma((T // PIECE, 4)),
+        dma, dma, dma, dma, dma, dma((5,)), dma, dma((2,)), dma, dma((T // PIECE, 4)), dma((4,)),
     ]
     result = pl.pallas_call(
         functools.partial(kernel, sizes),

time: 50.6 us -> 50.7 us (level)
  the two profiles are of different devices: /device:TPU:16 before, /device:TPU:2 now
where the time goes in v4:
time: 50.7 us; the launch traced here: 50.6 us
  Pallas kernels  49.7 us (98%)
  local copies, waits for them, and re-layouts  0.88 us (2%)
    pallas_call x1, Pallas kernels, per_device(): pl.pallas_call(functools.partial(kernel, sizes), out_shape=vmem((T, cols)...  49.7 us

profile of v4, /device:TPU:2, one launch (start us, length us, event | category | flops | bytes accessed | tf_op | source)
XLA Modules:
  0.0 50.6 jit_solution(4482649640050350522)
XLA Ops:
  0.0 49.7 %step.1 = f32[384,512]{1,0:T(8,128)S(1)} custom-call(bf16[384,2048]{1,0:T(8,128)(2,1)} %bitcast.8, bf16[8,128]{1,0:T(8,128)(2,1)} %cond.1, bf16[1,128]{1,0:T(2,128)(2,1)} %bitcast.13, bf16[3,64,128]{2,1,0:T(8,128)(2,1)} %bitcast.12, bf16[64,2048]{1,0:T(8,128)(2,1)} %bitcast.9, bf16[2048,256]{1,0:T(8,128)(2,1)} %qw.1, bf16[64,2048]{1,0:T(8,128)(2,1)} %bitcast.10, ...), custom_call_target="tpu_custom_call" | custom-call | tf_op jit(solution)/shard_map/step/pallas_call | solution.py:396
  49.7 0.9 %copy.13 = f32[1,384,512]{2,1,0:T(8,128)} copy(f32[1,384,512]{2,1,0:T(8,128)S(1)} %bitcast.7) | data formatting | bytes 1572864

commit v5 on v4

--- a/solution.py
+++ b/solution.py
@@ -47,7 +47,6 @@
 LATE = (3, 7, 8, -7)
 SLOT = {d: i for i, d in enumerate((0, *NEAR, 5, -5, *SOON, *LATE))}
 PIECE = 64
-Z_ROWS = 10
 
 
 def kernel(
@@ -55,7 +54,7 @@
     lat, cond, cctx, mod, ctx, qw, kw, vw, ow, sink, bias,
     out,
     xv, condv, cctxv, modv, cxv, qwv, owv, sinks, biass,
-    zsend, zrecv, gsend, grecv, gsum, ghave, xysend, xyrecv, vecs,
+    zsend, zcsend, zrecv, zcrecv, gsend, grecv, gsum, ghave, xysend, xyrecv, vecs,
     xn, cxn, xb, cxb, kvw, ct, st,
     kvc, kvx, qz, accw, mw, gath, mixed,
     in_sems,
@@ -101,8 +100,8 @@
     weights = modv[...].reshape(-1, modv.shape[2])
     rows = dot_t(act, weights)
     side = dot_t(act_c, weights[0:LANES])
-    zsend[0:samples, :] = rows[:, 0:LANES].astype(BF16)
-    zsend[samples:, :] = side[0:Z_ROWS - samples].astype(BF16)
+    zsend[...] = rows[:, 0:LANES]
+    zcsend[...] = side[0:1]
     gsend[...] = jnp.concatenate([rows[:half, LANES:], rows[half:, LANES:]], axis=1)
 
     def norm_rows(src, dst, rows):
@@ -116,11 +115,12 @@
         lax.fori_loop(0, src.shape[0] // rows, step, 0)
 
     pl.semaphore_wait(barrier, len(z_far) + len(xy_off))
-    for d in z_far:
-        pltpu.make_async_remote_copy(
-            src_ref=zsend, dst_ref=zrecv.at[d - 1], send_sem=z_send, recv_sem=z_recv,
-            device_id=z_at(d), device_id_type=MESH,
-        ).start()
+    for src, dst, i in ((zcsend, zcrecv, 1), (zsend, zrecv, 0)):
+        for d in z_far:
+            pltpu.make_async_remote_copy(
+                src_ref=src, dst_ref=dst.at[d - 1], send_sem=z_send.at[i], recv_sem=z_recv.at[i],
+                device_id=z_at(d), device_id_type=MESH,
+            ).start()
 
     loads[3].wait()
     norm_rows(xv, xn, REACH)
@@ -141,13 +141,16 @@
     loads[5].wait()
     loads[6].wait()
 
-    pltpu.make_async_copy(zrecv, zrecv, z_recv).wait()
-    total = zsend[...].astype(F32)
+    pltpu.make_async_copy(zcrecv, zcrecv, z_recv.at[1]).wait()
+    pltpu.make_async_copy(zrecv, zrecv, z_recv.at[0]).wait()
+    total = zsend[...]
+    total_c = zcsend[...]
     for d in range(SP - 1):
-        total = total + zrecv[d].astype(F32)
+        total = total + zrecv[d]
+        total_c = total_c + zcrecv[d]
     for s in range(samples):
         xysend[s, 0:1, :] = total[s:s + 1]
-        xysend[s, 1:2, :] = total[samples:samples + 1]
+        xysend[s, 1:2, :] = total_c[0:1]
     me = tp * DP + dp
     for t, d in sorted(xy_off, key=lambda o: -(min(o[0], TP - o[0]) + min(o[1], DP - o[1]) // 2)):
         target = lax.rem(dp + d, DP)
@@ -355,7 +358,8 @@
     pltpu.make_async_copy(others, others, y_send).wait()
     others = kvx.at[pl.ds(0, 2 * REACH), pl.ds(0, LANES)]
     pltpu.make_async_copy(others, others, h_send).wait()
-    pltpu.make_async_copy(zrecv, zrecv, z_send).wait()
+    pltpu.make_async_copy(zrecv, zrecv, z_send.at[0]).wait()
+    pltpu.make_async_copy(zcrecv, zcrecv, z_send.at[1]).wait()
     pltpu.make_async_copy(grecv, grecv, g_sems.at[0]).wait()
     others = ghave.at[pl.ds(0, DP - 1)]
     pltpu.make_async_copy(others, others, g_sems.at[2]).wait()
@@ -381,7 +385,7 @@
         vmem((T, D), BF16), vmem(cond.shape, BF16), vmem((1, cctx.shape[0]), BF16), vmem((mod.shape[0], mod.shape[2], mod.shape[1]), BF16),
         vmem((C, D), BF16), vmem(qw.shape, BF16), vmem(ow.shape, BF16),
         pltpu.SMEM(sink.shape, F32), pltpu.SMEM(bias.shape, F32),
-        vmem((Z_ROWS, LANES), BF16), vmem((SP - 1, Z_ROWS, LANES), BF16),
+        vmem((samples, LANES), F32), vmem((1, LANES), F32), vmem((SP - 1, samples, LANES), F32), vmem((SP - 1, 1, LANES), F32),
         vmem((samples // 2, LANES), F32), vmem((SP - 1, samples // 2, LANES), F32), vmem((samples // 2, LANES), F32),
         vmem((DP, samples // 2, LANES), F32),
         vmem((samples, 2, LANES), F32), vmem((TP * DP, 2, LANES), F32), vmem((2, TP * DP // 2, 2, LANES), F32),
@@ -391,7 +395,7 @@
         vmem((heads, T, 2 * LANES), F32), vmem((heads, T, LANES), F32),
         vmem((TP, T, width), BF16), vmem((T, cols), F32),
         dma((11,)),
-        dma, dma, dma, dma, dma, dma((5,)), dma, dma((2,)), dma, dma((T // PIECE, 4)), dma((4,)),
+        dma((2,)), dma((2,)), dma, dma, dma, dma((5,)), dma, dma((2,)), dma, dma((T // PIECE, 4)), dma((4,)),
     ]
     result = pl.pallas_call(
         functools.partial(kernel, sizes),

time: 50.7 us -> 50.7 us (level)
  the two profiles are of different devices: /device:TPU:2 before, /device:TPU:32 now
where the time goes in v5:
time: 50.7 us; the launch traced here: 50.6 us
  Pallas kernels  49.7 us (98%)
  local copies, waits for them, and re-layouts  0.88 us (2%)
    pallas_call x1, Pallas kernels, per_device(): pl.pallas_call(functools.partial(kernel, sizes), out_shape=vmem((T, cols)...  49.7 us

profile of v5, /device:TPU:32, one launch (start us, length us, event | category | flops | bytes accessed | tf_op | source)
XLA Modules:
  0.0 50.6 jit_solution(11904125036784836123)
XLA Ops:
  0.0 49.7 %step.1 = f32[384,512]{1,0:T(8,128)S(1)} custom-call(bf16[384,2048]{1,0:T(8,128)(2,1)} %bitcast.8, bf16[8,128]{1,0:T(8,128)(2,1)} %cond.1, bf16[1,128]{1,0:T(2,128)(2,1)} %bitcast.13, bf16[3,64,128]{2,1,0:T(8,128)(2,1)} %bitcast.12, bf16[64,2048]{1,0:T(8,128)(2,1)} %bitcast.9, bf16[2048,256]{1,0:T(8,128)(2,1)} %qw.1, bf16[64,2048]{1,0:T(8,128)(2,1)} %bitcast.10, ...), custom_call_target="tpu_custom_call" | custom-call | tf_op jit(solution)/shard_map/step/pallas_call | solution.py:400
  49.8 0.9 %copy.13 = f32[1,384,512]{2,1,0:T(8,128)} copy(f32[1,384,512]{2,1,0:T(8,128)S(1)} %bitcast.7) | data formatting | bytes 1572864

commit v6 on v5

--- a/solution.py
+++ b/solution.py
@@ -54,7 +54,7 @@
     lat, cond, cctx, mod, ctx, qw, kw, vw, ow, sink, bias,
     out,
     xv, condv, cctxv, modv, cxv, qwv, owv, sinks, biass,
-    zsend, zcsend, zrecv, zcrecv, gsend, grecv, gsum, ghave, xysend, xyrecv, vecs,
+    zsend, zcsend, zrecv, zcrecv, gsend, grecv, gsum, ghave, xysend, xyrecv, xycsend, xycrecv, vecs,
     xn, cxn, xb, cxb, kvw, ct, st,
     kvc, kvx, qz, accw, mw, gath, mixed,
     in_sems,
@@ -141,37 +141,50 @@
     loads[5].wait()
     loads[6].wait()
 
+    me = tp * DP + dp
+    xy_order = sorted(xy_off, key=lambda o: -(min(o[0], TP - o[0]) + min(o[1], DP - o[1]) // 2))
+
+    def xy_copy(src, dst, t, target, i):
+        return pltpu.make_async_remote_copy(
+            src_ref=src, dst_ref=dst.at[me], send_sem=xy_send.at[i], recv_sem=xy_recv.at[i],
+            device_id={"tp": lax.rem(tp + t, TP), "dp": target}, device_id_type=MESH,
+        )
+
     pltpu.make_async_copy(zcrecv, zcrecv, z_recv.at[1]).wait()
+    total_c = zcsend[...]
+    for d in range(SP - 1):
+        total_c = total_c + zcrecv[d]
+    xycsend[...] = total_c
+    for t, d in xy_order:
+        xy_copy(xycsend, xycrecv, t, lax.rem(dp + d, DP), 1).start()
+    xycrecv[me] = total_c
     pltpu.make_async_copy(zrecv, zrecv, z_recv.at[0]).wait()
     total = zsend[...]
-    total_c = zcsend[...]
     for d in range(SP - 1):
         total = total + zrecv[d]
-        total_c = total_c + zcrecv[d]
     for s in range(samples):
-        xysend[s, 0:1, :] = total[s:s + 1]
-        xysend[s, 1:2, :] = total_c[0:1]
-    me = tp * DP + dp
-    for t, d in sorted(xy_off, key=lambda o: -(min(o[0], TP - o[0]) + min(o[1], DP - o[1]) // 2)):
+        xysend[s] = total[s:s + 1]
+    for t, d in xy_order:
         target = lax.rem(dp + d, DP)
-        pltpu.make_async_remote_copy(
-            src_ref=xysend.at[target], dst_ref=xyrecv.at[me], send_sem=xy_send, recv_sem=xy_recv,
-            device_id={"tp": lax.rem(tp + t, TP), "dp": target}, device_id_type=MESH,
-        ).start()
+        xy_copy(xysend.at[target], xyrecv, t, target, 0).start()
     xyrecv[me] = xysend[dp]
     for d in z_far:
         pltpu.make_async_remote_copy(
             src_ref=gsend, dst_ref=grecv.at[d - 1], send_sem=g_sems.at[0], recv_sem=g_sems.at[1],
             device_id=z_at(d), device_id_type=MESH,
         ).start()
-    others = xyrecv.at[pl.ds(0, len(xy_off))]
-    pltpu.make_async_copy(others, others, xy_recv).wait()
-    chunks = vecs.shape[1]
-    low2 = lane_iota((2, LANES)) < 64
-    for k in range(chunks):
-        left, right = xyrecv[2 * k], xyrecv[2 * k + 1]
-        vecs[0, k] = jnp.where(low2, left, pltpu.roll(right, 64, 1))
-        vecs[1, k] = jnp.where(low2, pltpu.roll(left, 64, 1), right) + 1.0
+    chunks = vecs.shape[2]
+    low1 = lane_iota((1, LANES)) < 64
+
+    def vectors(which, got, i):
+        others = got.at[pl.ds(0, len(xy_off))]
+        pltpu.make_async_copy(others, others, xy_recv.at[i]).wait()
+        for k in range(chunks):
+            left, right = got[2 * k], got[2 * k + 1]
+            vecs[which, 0, k] = jnp.where(low1, left, pltpu.roll(right, 64, 1))
+            vecs[which, 1, k] = jnp.where(low1, pltpu.roll(left, 64, 1), right) + 1.0
+
+    vectors(1, xycrecv, 1)
 
     def ctx_at(d, count=1):
         return kvc.at[pl.ds(SLOT[d] * C, count * C), pl.ds(0, LANES)]
@@ -184,14 +197,15 @@
 
     for k in range(chunks):
         c = slice(k * LANES, (k + 1) * LANES)
-        cxb[:, c] = (cxn[:, c] * vecs[1, k, 1:2, :] + vecs[0, k, 1:2, :]).astype(BF16)
+        cxb[:, c] = (cxn[:, c] * vecs[1, 1, k] + vecs[1, 0, k]).astype(BF16)
     kvc[0:C, 0:LANES] = dot_t(cxb[...], kvw[...]).astype(BF16)
     for d in DIRECT:
         ctx_copy(0, d, d, {5: 1, -5: 2}.get(d, 0)).start()
 
+    vectors(0, xyrecv, 0)
     def modulate(k, _):
         c = pl.ds(pl.multiple_of(k * LANES, LANES), LANES)
-        xb[:, c] = (xn[:, c] * vecs[1, k, 0:1, :] + vecs[0, k, 0:1, :]).astype(BF16)
+        xb[:, c] = (xn[:, c] * vecs[0, 1, k] + vecs[0, 0, k]).astype(BF16)
         return 0
 
     lax.fori_loop(0, chunks, modulate, 0)
@@ -336,7 +350,6 @@
 
     others = ghave.at[pl.ds(0, DP - 1)]
     pltpu.make_async_copy(others, others, g_sems.at[3]).wait()
-    low1 = lane_iota((1, LANES)) < 64
     gate_chunks = []
     for k in range(DP // 2):
         left, right = (ghave[2 * k + i, pl.ds(lax.rem(dp, half), 1), :] for i in range(2))
@@ -363,8 +376,9 @@
     pltpu.make_async_copy(grecv, grecv, g_sems.at[0]).wait()
     others = ghave.at[pl.ds(0, DP - 1)]
     pltpu.make_async_copy(others, others, g_sems.at[2]).wait()
-    others = xyrecv.at[pl.ds(0, len(xy_off))]
-    pltpu.make_async_copy(others, others, xy_send).wait()
+    for i in range(2):
+        others = xyrecv.at[pl.ds(0, len(xy_off))]
+        pltpu.make_async_copy(others, others, xy_send.at[i]).wait()
     others = kvc.at[pl.ds(C, (SP - 1) * C), pl.ds(0, LANES)]
     pltpu.make_async_copy(others, others, c_send).wait()
 
@@ -388,14 +402,15 @@
         vmem((samples, LANES), F32), vmem((1, LANES), F32), vmem((SP - 1, samples, LANES), F32), vmem((SP - 1, 1, LANES), F32),
         vmem((samples // 2, LANES), F32), vmem((SP - 1, samples // 2, LANES), F32), vmem((samples // 2, LANES), F32),
         vmem((DP, samples // 2, LANES), F32),
-        vmem((samples, 2, LANES), F32), vmem((TP * DP, 2, LANES), F32), vmem((2, TP * DP // 2, 2, LANES), F32),
+        vmem((samples, 1, LANES), F32), vmem((TP * DP, 1, LANES), F32), vmem((1, LANES), F32),
+        vmem((TP * DP, 1, LANES), F32), vmem((2, 2, TP * DP // 2, 1, LANES), F32),
         vmem((T, D), F32), vmem((C, D), F32), vmem((T, D), BF16), vmem((C, D), BF16), vmem((LANES, D), BF16),
         vmem((T, LANES), F32), vmem((T, LANES), F32),
         vmem((SP * C, 2 * LANES), BF16), vmem((T + 2 * REACH, 2 * LANES), BF16), vmem((heads, T, LANES), BF16),
         vmem((heads, T, 2 * LANES), F32), vmem((heads, T, LANES), F32),
         vmem((TP, T, width), BF16), vmem((T, cols), F32),
         dma((11,)),
-        dma((2,)), dma((2,)), dma, dma, dma, dma((5,)), dma, dma((2,)), dma, dma((T // PIECE, 4)), dma((4,)),
+        dma((2,)), dma((2,)), dma((2,)), dma((2,)), dma, dma((5,)), dma, dma((2,)), dma, dma((T // PIECE, 4)), dma((4,)),
     ]
     result = pl.pallas_call(
         functools.partial(kernel, sizes),

time: 50.7 us -> 50.8 us (level)
  the two profiles are of different devices: /device:TPU:32 before, /device:TPU:2 now
where the time goes in v6:
time: 50.8 us; the launch traced here: 50.7 us
  Pallas kernels  49.8 us (98%)
  local copies, waits for them, and re-layouts  0.88 us (2%)
    pallas_call x1, Pallas kernels, per_device(): pl.pallas_call(functools.partial(kernel, sizes), out_shape=vmem((T, cols)...  49.8 us

profile of v6, /device:TPU:2, one launch (start us, length us, event | category | flops | bytes accessed | tf_op | source)
XLA Modules:
  0.0 50.7 jit_solution(5973618667294691718)
XLA Ops:
  0.0 49.8 %step.1 = f32[384,512]{1,0:T(8,128)S(1)} custom-call(bf16[384,2048]{1,0:T(8,128)(2,1)} %bitcast.8, bf16[8,128]{1,0:T(8,128)(2,1)} %cond.1, bf16[1,128]{1,0:T(2,128)(2,1)} %bitcast.13, bf16[3,64,128]{2,1,0:T(8,128)(2,1)} %bitcast.12, bf16[64,2048]{1,0:T(8,128)(2,1)} %bitcast.9, bf16[2048,256]{1,0:T(8,128)(2,1)} %qw.1, bf16[64,2048]{1,0:T(8,128)(2,1)} %bitcast.10, ...), custom_call_target="tpu_custom_call" | custom-call | tf_op jit(solution)/shard_map/step/pallas_call | solution.py:415
  49.8 0.9 %copy.13 = f32[1,384,512]{2,1,0:T(8,128)} copy(f32[1,384,512]{2,1,0:T(8,128)S(1)} %bitcast.7) | data formatting | bytes 1572864
